TPU v7x, 32 devices: a whole 2x2x4 slice. The times are simulated.
32 devices in a mesh: sp: 8 (over z, y), tp: 4 (over x, core).
Axes of the slice: x: 2, y: 2, z: 4, core: 2. Of those that a mesh axis runs over, the one named last changes fastest.
Arguments:
- resid: bfloat16 [6144, 4096], P(('sp', 'tp')), may hold values from -80 to 80
- pool_in: bfloat16 [6144, 1024], P('sp', 'tp'), may hold values from -6 to 6
- pool_weight: bfloat16 [4, 256, 256], P('tp'), may hold values from -0.375 to 0.375
- pool_scale: float32 [1024], P('tp'), may hold values from 0.1 to 1.9
- out_weight: bfloat16 [1024, 4096], P('tp'), may hold values from -0.1875 to 0.1875
- norm_gain: float32 [4096], replicated, may hold values from 0.1 to 1.9
- route_ids: int32 [6144, 4], P(('sp', 'tp')), may hold values from 0 to 31, all different within a row; in each aligned block of 192 rows (0 to 191, 192 to 383, ...) at most 36 rows name the same one
- route_weight: float32 [6144, 4], P(('sp', 'tp')), may hold values from 0.1 to 1
- expert_gate: bfloat16 [32, 4096, 384], P('sp'), may hold values from -0.09375 to 0.09375
- expert_up: bfloat16 [32, 4096, 384], P('sp'), may hold values from -0.09375 to 0.09375
- expert_down: bfloat16 [32, 384, 4096], P('sp'), may hold values from -0.3125 to 0.3125
- shared_gate: bfloat16 [4096, 384], replicated, may hold values from -0.09375 to 0.09375
- shared_up: bfloat16 [4096, 384], replicated, may hold values from -0.09375 to 0.09375
- shared_down: bfloat16 [384, 4096], replicated, may hold values from -0.3125 to 0.3125
Outputs:
- layer_out: bfloat16 [6144, 4096], P(('sp', 'tp'))
Inputs may be any that keep to these rules, and one draw needn't show every extreme that they name: `route_ids`: each row names 4 different experts. Among the rows of one device no expert is named more than 36 times, and that count is reached.
All inputs are finite; a program needn't handle non-finite values.
Results may differ from a plain program's by a relative error of at most 0.012.
Values may be sent and summed in bfloat16 or wider, within the bound.
No kernel may reach another device: no remote copies, remote signals or barrier semaphores. Data moves between devices by JAX's collectives and lax.ppermute only.
A program may use at most 192 MiB of HBM per device.

v0:
```python
import functools

import jax
import jax.numpy as jnp
from jax import lax
from jax.experimental import pallas as pl
from jax.experimental.pallas import tpu as pltpu
from jax.sharding import PartitionSpec as P


reach_rows = 8
norm_eps = 1e-06
outer = 4


f32 = jnp.float32
bf16 = jnp.bfloat16


def with_halo(cells, axis, width):
    count = lax.axis_size(axis)
    ends = count - 1
    head = cells[:width]
    tail = cells[cells.shape[0] - width :]
    return jnp.concatenate(
        [
            lax.ppermute(tail, axis, [(i, i + 1) for i in range(ends)]),
            cells,
            lax.ppermute(head, axis, [(i + 1, i) for i in range(ends)]),
        ],
        axis=0,
    )


def window_means(padded, length, offset, whole_len):
    positions = offset + lax.iota(jnp.int32, length)
    running = jnp.zeros((length,) + padded.shape[1:], f32)
    averages = []
    covered = 0
    for section_num in range(4):
        half_span = 2**section_num
        for row_shift in list(range(-half_span, -covered)) + list(range(covered, half_span)):
            running = running + padded[reach_rows + row_shift : reach_rows + row_shift + length]
        covered = half_span
        upper_end = jnp.minimum(positions + half_span, whole_len)
        lower_end = jnp.maximum(positions - half_span, 0)
        row_count = (upper_end - lower_end).astype(f32)
        averages.append(running / row_count[:, None, None])
    return averages


def pool_mix(pool_in, pool_weight, pool_scale):
    tok_local = pool_in.shape[0]
    local_groups, group_width = pool_weight.shape[:2]
    padded = with_halo(pool_in, "sp", reach_rows).astype(f32)
    padded = padded.reshape(tok_local + 2 * reach_rows, local_groups, group_width)
    averages = window_means(
        padded, tok_local, lax.axis_index("sp") * tok_local, tok_local * lax.axis_size("sp")
    )
    center = padded[reach_rows : reach_rows + tok_local]
    group_ids = lax.axis_index("tp") * local_groups + lax.iota(jnp.int32, local_groups)
    chosen = averages[0]
    for section_num in range(1, 4):
        chosen = jnp.where((group_ids == section_num)[None, :, None], averages[section_num], chosen)
    spread = (chosen - center).astype(bf16)
    mixed_rows = jnp.einsum("tgc,gce->tge", spread, pool_weight, preferred_element_type=f32)
    return (mixed_rows.reshape(tok_local, -1) * pool_scale[None, :]).astype(bf16)


def out_norm_kernel(blocks, keep, pick, *refs):
    plane, refs = refs[0], refs[1:]
    pools, resids = refs[:blocks], refs[blocks : 2 * blocks]
    refs = refs[2 * blocks :]
    gain, weights, outs = refs[0], refs[1:5], refs[5:]
    width = gain.shape[1]
    depth = weights[0].shape[0]
    step = 1024
    steps = width // step

    def part(n):
        return pl.ds(pl.multiple_of(n * step, step), step)

    for i in range(blocks):
        pool, resid = pools[i], resids[i]
        normed = outs[i]
        middle = outs[blocks] if keep and i == 0 else normed

        def project(n, total):
            at = part(n)
            acc = resid[:, at].astype(f32)
            for j, weight in enumerate(weights):
                acc = acc + jnp.dot(
                    pool[:, j * depth : (j + 1) * depth],
                    weight[:, at],
                    preferred_element_type=f32,
                )
            mid = acc.astype(bf16)
            middle[:, at] = mid
            mid = mid.astype(f32)
            return total + jnp.sum(mid * mid, axis=1, keepdims=True)

        total = lax.fori_loop(0, steps, project, jnp.zeros((resid.shape[0], 1), f32))
        scale = lax.rsqrt(total * (1.0 / width) + norm_eps)

        def finish(n, carry):
            at = part(n)
            value = (middle[:, at].astype(f32) * scale * gain[:, at]).astype(bf16)
            normed[:, at] = value
            if pick:
                near, spare = outs[blocks], outs[blocks + 1]
                low = plane[0] <= 1

                @pl.when(low if i == 1 else jnp.logical_not(low))
                def _():
                    near[:, at] = value

                @pl.when(plane[0] == 1 + i)
                def _():
                    spare[:, at] = value

                if i == 0:

                    @pl.when((plane[0] != 1) & (plane[0] != 2))
                    def _():
                        spare[:, at] = jnp.zeros_like(value)

            return carry

        lax.fori_loop(0, steps, finish, 0)


def out_norm(pools, resids, gain, weights, plane, keep, pick):
    blocks = len(pools)
    vm = pl.BlockSpec(memory_space=pltpu.VMEM)
    shapes = [jax.ShapeDtypeStruct(r.shape, bf16) for r in resids]
    shapes += [shapes[0]] * (1 if keep else 2 if pick else 0)
    rows = sum(r.shape[0] for r in resids)
    return pl.pallas_call(
        functools.partial(out_norm_kernel, blocks, keep, pick),
        out_shape=shapes,
        in_specs=[pl.BlockSpec(memory_space=pltpu.SMEM)]
        + [vm] * (2 * blocks + 1 + len(weights)),
        out_specs=[vm] * len(shapes),
        compiler_params=pltpu.CompilerParams(vmem_limit_bytes=40 * 2**20),
        cost_estimate=pl.CostEstimate(
            flops=2 * rows * pools[0].shape[1] * gain.shape[0],
            bytes_accessed=4 * rows * gain.shape[0],
            transcendentals=rows,
        ),
        name="out_norm",
    )(plane.reshape(1), *pools, *resids, gain.reshape(1, -1), *weights)


def combine_kernel(count, own, *refs):
    mixes, parts, out = refs[:count], refs[count : 2 * count], refs[2 * count]
    total = own[...]
    for mix, part in zip(mixes, parts):
        total = total + lax.dot_general(
            mix[...], part[...], (((0,), (0,)), ((), ())), preferred_element_type=f32
        )
    out[...] = total.astype(bf16)


def combine(own, mixes, parts):
    count = len(parts)
    rows, width = own.shape
    step = width // 4
    whole = [pl.BlockSpec(m.shape, lambda n: (0, 0)) for m in mixes]
    cut = [pl.BlockSpec((p.shape[0], step), lambda n: (0, n)) for p in parts]
    mine = pl.BlockSpec((rows, step), lambda n: (0, n))
    return pl.pallas_call(
        functools.partial(combine_kernel, count),
        grid=(4,),
        out_shape=jax.ShapeDtypeStruct(own.shape, bf16),
        in_specs=[mine] + whole + cut,
        out_specs=mine,
        compiler_params=pltpu.CompilerParams(vmem_limit_bytes=24 * 2**20),
        cost_estimate=pl.CostEstimate(
            flops=2 * rows * width * sum(p.shape[0] for p in parts),
            bytes_accessed=8 * rows * width,
            transcendentals=0,
        ),
        name="combine",
    )(own, *mixes, *parts)


def expert_kernel(peers, capacity, pad, *refs):
    line, others, refs = refs[0], refs[1 : 1 + peers], refs[1 + peers :]
    rank, share, gate, up, down, own = refs[:6]
    backs = refs[6 : 6 + peers]
    packed, made, pick, mixing, shift = refs[6 + peers :]
    expert = pl.program_id(0)
    count = pl.num_programs(0)
    experts = rank.shape[0]
    rows = line.shape[0]
    other_rows = others[0].shape[0]

    @pl.when(expert == 0)
    def _():
        seat = lax.broadcasted_iota(jnp.int32, (pad, rows), 0).astype(f32)
        seat = jnp.where(seat < capacity, seat, -2.0)
        row = lax.broadcasted_iota(jnp.int32, (pad, other_rows), 0)
        col = lax.broadcasted_iota(jnp.int32, (pad, other_rows), 1)
        for e in range(experts):
            here = slice(e * pad, (e + 1) * pad)
            hit = rank[e : e + 1, :] == seat
            pick[here, :] = hit.astype(f32).astype(bf16)
            mixing[here, :] = jnp.where(hit, share[e : e + 1, :], 0.0).astype(bf16)
            shift[here, :] = (
                ((col == e * capacity + row) & (row < capacity)).astype(f32).astype(bf16)
            )
        for i in range(1 + peers):
            if i == 0:
                moved = jnp.dot(pick[...], line[...], preferred_element_type=f32)
            else:
                moved = jnp.dot(shift[...], others[i - 1][...], preferred_element_type=f32)
            moved = moved.astype(bf16)
            for e in range(experts):
                packed[e, i * pad : (i + 1) * pad, :] = moved[e * pad : (e + 1) * pad]

    tokens = packed[expert]
    gated = jnp.dot(tokens, gate[0], preferred_element_type=f32)
    lifted = jnp.dot(tokens, up[0], preferred_element_type=f32)
    hidden = (gated * (1.0 / (1.0 + jnp.exp(-gated))) * lifted).astype(bf16)
    result = jnp.dot(hidden, down[0], preferred_element_type=f32).astype(bf16)
    for i in range(1 + peers):
        made[i, pl.ds(pl.multiple_of(expert * pad, pad), pad), :] = result[i * pad : (i + 1) * pad]

    @pl.when(expert == count - 1)
    def _():
        rows_in = (((0,), (0,)), ((), ()))
        own[...] = lax.dot_general(mixing[...], made[0], rows_in, preferred_element_type=f32)
        for j in range(peers):
            backs[j][...] = lax.dot_general(
                shift[...], made[1 + j], rows_in, preferred_element_type=f32
            ).astype(bf16)


def run_experts(line, others, rank, share, gate, up, down, capacity):
    peers = len(others)
    experts, width, hidden = gate.shape
    pad = -(-capacity // 16) * 16
    rows = line.shape[0]
    vm = pl.BlockSpec(memory_space=pltpu.VMEM)

    def per_expert(a):
        return pl.BlockSpec((1,) + a.shape[1:], lambda e: (e, 0, 0))

    back_shape = jax.ShapeDtypeStruct(others[0].shape, bf16)
    filled = (1 + peers) * pad
    outs = pl.pallas_call(
        functools.partial(expert_kernel, peers, capacity, pad),
        grid=(experts,),
        out_shape=[jax.ShapeDtypeStruct(line.shape, f32)] + [back_shape] * peers,
        in_specs=[vm] * (3 + peers) + [per_expert(a) for a in (gate, up, down)],
        out_specs=[vm] * (1 + peers),
        scratch_shapes=[
            pltpu.VMEM((experts, filled, width), bf16),
            pltpu.VMEM((1 + peers, experts * pad, width), bf16),
            pltpu.VMEM((experts * pad, rows), bf16),
            pltpu.VMEM((experts * pad, rows), bf16),
            pltpu.VMEM((experts * pad, others[0].shape[0]), bf16),
        ],
        compiler_params=pltpu.CompilerParams(
            vmem_limit_bytes=48 * 2**20, dimension_semantics=("arbitrary",)
        ),
        cost_estimate=pl.CostEstimate(
            flops=6 * experts * filled * width * hidden,
            bytes_accessed=6 * experts * width * hidden,
            transcendentals=experts * filled * hidden,
        ),
        name="experts",
    )(line, *others, rank, share, gate, up, down)
    return outs[0], outs[1:]


def shards(
    resid,
    pool_in,
    pool_weight,
    pool_scale,
    out_weight,
    norm_gain,
    route_ids,
    route_weight,
    expert_gate,
    expert_up,
    expert_down,
    shared_gate,
    shared_up,
    shared_down,
):
    n_sp, n_tp = lax.axis_size("sp"), lax.axis_size("tp")
    inner = n_sp // outer
    plane = lax.axis_index("sp") // inner
    lane = lax.axis_index("sp") % inner
    mine = lax.axis_index("tp")
    rows_here, top_count = route_ids.shape
    experts_here = expert_gate.shape[0]
    expert_total = experts_here * n_sp
    capacity = rows_here * top_count * 3 // (2 * expert_total)

    def along_outer(x, pairs):
        pairs = [(a * inner + i, b * inner + i) for a, b in pairs for i in range(inner)]
        return lax.ppermute(x, "sp", pairs)

    def along_inner(x, by):
        pairs = [
            (a * inner + i, a * inner + (i + by) % inner)
            for a in range(outer)
            for i in range(inner)
        ]
        return lax.ppermute(x, "sp", pairs)

    def along_tp(x, bits):
        return lax.ppermute(x, "tp", [(i, i ^ bits) for i in range(n_tp)])

    ups = [(0, 1), (1, 2), (2, 3)]
    downs = [(3, 2), (2, 1), (1, 0)]

    weights = [out_weight, along_tp(out_weight, 1), along_tp(out_weight, 2)]
    weights.append(along_tp(weights[2], 1))
    resid_up = along_outer(resid, ups)
    resid_down = along_outer(resid, downs)

    ids = route_ids.T
    chosen = route_weight.T
    numbers = lax.iota(jnp.int32, expert_total)[:, None]
    member = jnp.zeros((expert_total, rows_here), jnp.bool_)
    share = jnp.zeros((expert_total, rows_here), f32)
    for k in range(top_count):
        hit = ids[k][None, :] == numbers
        member = member | hit
        share = share + jnp.where(hit, chosen[k][None, :], 0.0)
    order = lax.iota(jnp.int32, rows_here)
    ahead = (order[:, None] < order[None, :]).astype(bf16)
    seat = jnp.dot(member.astype(bf16), ahead, preferred_element_type=f32)
    seat = jnp.where(member, seat, -1.0)
    per_plane = inner * experts_here
    table = jnp.stack(
        [seat.reshape(outer, per_plane, rows_here), share.reshape(outer, per_plane, rows_here)],
        axis=1,
    )

    def table_for(by):
        return lax.dynamic_index_in_dim(table, lax.rem(plane + by, outer), axis=0, keepdims=False)

    tables = [table_for(0)]
    for by in range(1, outer):
        tables.append(along_outer(table_for(by), [(a, (a + by) % outer) for a in range(outer)]))
    low = plane <= 1
    slot_tables = [
        tables[0],
        jnp.where(low, tables[3], tables[1]),
        tables[2],
        jnp.where(low, tables[1], tables[3]),
    ]
    slots = range(4)
    peers = range(1, inner)

    def group_of(slot, by):
        start = lax.rem(lane + by, inner) * experts_here
        return lax.dynamic_slice_in_dim(slot_tables[slot], start, experts_here, axis=1)

    seats_out = experts_here * capacity
    line_no = lax.iota(jnp.int32, seats_out)
    spreader = (
        lax.div(line_no, capacity)[:, None] == lax.iota(jnp.int32, experts_here)[None, :]
    ).astype(bf16)
    seat_no = lax.rem(line_no, capacity).astype(f32)[:, None]
    send_pick = [[] for _ in slots]
    send_mix = [[] for _ in slots]
    for k in slots:
        for j in peers:
            t = group_of(k, j).astype(bf16)
            wide_rank = jnp.dot(spreader, t[0], preferred_element_type=f32)
            wide_share = jnp.dot(spreader, t[1], preferred_element_type=f32)
            hit = wide_rank == seat_no
            send_pick[k].append(hit.astype(bf16))
            send_mix[k].append(jnp.where(hit, wide_share, 0.0).astype(bf16))

    def exchange(slot, rows):
        got = []
        for j in peers:
            sent = jnp.dot(send_pick[slot][j - 1], rows, preferred_element_type=f32).astype(bf16)
            got.append(along_inner(sent, j))
        return got

    other_resid = exchange(0, resid)

    pooled = pool_mix(pool_in, pool_weight, pool_scale)

    def pooled_for(bits):
        return lax.dynamic_slice_in_dim(pooled, (mine ^ bits) * rows_here, rows_here, axis=0)

    pieces = [pooled_for(0)] + [along_tp(pooled_for(b), b) for b in range(1, n_tp)]
    pooled = jnp.concatenate(pieces, axis=1)
    pooled_up = along_outer(pooled, ups)
    pooled_down = along_outer(pooled, downs)
    other_pooled = exchange(0, pooled)

    up1, down1, near, spare = out_norm(
        [pooled_up, pooled_down],
        [resid_up, resid_down],
        norm_gain,
        weights,
        plane,
        False,
        True,
    )
    normed, *other_normed, middle = out_norm(
        [pooled, *other_pooled], [resid, *other_resid], norm_gain, weights, plane, True, False
    )

    up2 = along_outer(up1, ups[1:])
    down2 = along_outer(down1, downs[1:])
    up3 = along_outer(up2, ups[2:])
    down3 = along_outer(down2, downs[2:])
    lines = [normed, near, up2 + down2, spare + up3 + down3]
    arrived = [other_normed] + [exchange(k, lines[k]) for k in (1, 2, 3)]
    owns, backs = [], []
    for k in slots:
        own_table = group_of(k, 0)
        own, back = run_experts(
            lines[k],
            arrived[k],
            own_table[0],
            own_table[1],
            expert_gate,
            expert_up,
            expert_down,
            capacity,
        )
        owns.append(own)
        backs.append(back)

    def partial_sum(k):
        parts = [along_inner(backs[k][j - 1], -j) for j in peers]
        return combine(owns[k], send_mix[k], parts)

    sums = [partial_sum(k) for k in slots]

    shared_hidden = (
        jax.nn.silu(jnp.dot(normed, shared_gate, preferred_element_type=f32))
        * jnp.dot(normed, shared_up, preferred_element_type=f32)
    ).astype(bf16)
    base = middle.astype(f32) + jnp.dot(
        shared_hidden, shared_down, preferred_element_type=f32
    )

    got_up = along_outer(sums[3], ups[:1])
    got_down = along_outer(sums[3], downs[:1])
    mid = sums[2] + got_up + got_down
    got_up = along_outer(mid, ups[:2])
    got_down = along_outer(mid, downs[:2])
    near_up = jnp.where(plane == 2, sums[3], sums[1]) + got_up
    near_down = jnp.where(plane == 1, sums[3], sums[1]) + got_down
    got_up = along_outer(near_up, ups)
    got_down = along_outer(near_down, downs)
    base = base + sums[0].astype(f32)
    return (base + got_up.astype(f32) + got_down.astype(f32)).astype(bf16)


def solution(mesh):
    return jax.shard_map(
        shards,
        mesh=mesh,
        in_specs=(
            P(("sp", "tp"), None),
            P("sp", "tp"),
            P("tp", None, None),
            P("tp"),
            P("tp", None),
            P(),
            P(("sp", "tp"), None),
            P(("sp", "tp"), None),
            P("sp", None, None),
            P("sp", None, None),
            P("sp", None, None),
            P(),
            P(),
            P(),
        ),
        out_specs=P(("sp", "tp"), None),
        check_vma=False,
    )
```

profile of v0, /device:TPU:0, one launch (start us, length us, event | category | flops | bytes accessed | tf_op | source)
XLA Modules:
  0.0 481.2 jit_solution(7446825682745258163)
XLA Ops:
  0.0 3.0 collective-permute-start.8
  3.0 4.7 collective-permute-start.13
  11.0 4.5 collective-permute-start
  17.9 31.0 %collective-permute-done.8.refs_8_ = bf16[256,4096]{1,0:T(8,128)(2,1)} collective-permute-done((bf16[256,4096]{1,0:T(8,128)(2,1)}, bf16[256,4096]{1,0:T(8,128)(2,1)}, u32[]{:S(2)}, u32[]{:S(2)}) %collective-permute-start.8) | collective-permute-done | bytes 2097184 | tf_op jit(solution)/shard_map/ppermute | solution.py:316
  58.0 3.6 collective-permute-done.3
  62.9 3.6 collective-permute-start.11
  66.5 8.6 %collective-permute-done.11.refs_1_ = bf16[192,1024]{1,0:T(8,128)(2,1)S(1)} collective-permute-done((bf16[192,1024]{1,0:T(8,128)(2,1)S(1)}, bf16[192,1024]{1,0:T(8,128)(2,1)S(1)}, u32[]{:S(2)}, u32[]{:S(2)}) %collective-permute-start.11) | collective-permute-done | bytes 393248 | tf_op jit(solution)/shard_map/ppermute | solution.py:305
  77.3 11.8 %collective-permute-done.12.refs_2_ = bf16[192,1024]{1,0:T(8,128)(2,1)} collective-permute-done((bf16[192,1024]{1,0:T(8,128)(2,1)S(1)}, bf16[192,1024]{1,0:T(8,128)(2,1)}, u32[]{:S(2)}, u32[]{:S(2)}) %collective-permute-start.12) | collective-permute-done | bytes 393248 | tf_op jit(solution)/shard_map/ppermute | solution.py:305
  91.6 12.2 %out_norm.3 = (bf16[192,4096]{1,0:T(8,128)(2,1)}, bf16[192,4096]{1,0:T(8,128)(2,1)}, bf16[192,4096]{1,0:T(8,128)(2,1)S(1)}, bf16[192,4096]{1,0:T(8,128)(2,1)S(1)}) custom-call(s32[1]{0:T(128)} %bitcast.refs_0_, bf16[192,1024]{1,0:T(8,128)(2,1)S(1)} %copy-done.18, bf16[192,1024]{1,0:T(8,128)(2,1)} %collective-permute-done.12.refs_2_, ...), custom_call_target="tpu_custom_call" | custom-call | flops 3221225472 | bytes 6291456 | tf_op jit(solution)/shard_map/out_norm/pallas_call | solution.py:138
  110.2 33.2 %collective-permute-done.17 = bf16[192,4096]{1,0:T(8,128)(2,1)} collective-permute-done((bf16[192,4096]{1,0:T(8,128)(2,1)}, bf16[192,4096]{1,0:T(8,128)(2,1)}, u32[]{:S(2)}, u32[]{:S(2)}) %collective-permute-start.17) | collective-permute-done | bytes 1572896 | tf_op jit(solution)/shard_map/ppermute | solution.py:305
  148.9 3.6 collective-permute-start.20
  153.7 26.8 %collective-permute-done.20 = f32[2,8,192]{2,1,0:T(8,128)} collective-permute-done((f32[2,8,192]{2,1,0:T(8,128)}, f32[2,8,192]{2,1,0:T(8,128)}, u32[]{:S(2)}, u32[]{:S(2)}) %collective-permute-start.20) | collective-permute-done | bytes 12320 | tf_op jit(solution)/shard_map/ppermute | solution.py:305
  189.5 3.1 collective-permute-start.25
  199.5 13.7 %collective-permute-done.21.refs_1_ = bf16[144,4096]{1,0:T(8,128)(2,1)} collective-permute-done((bf16[144,4096]{1,0:T(8,128)(2,1)}, bf16[144,4096]{1,0:T(8,128)(2,1)}, u32[]{:S(2)}, u32[]{:S(2)}) %collective-permute-start.21) | collective-permute-done | bytes 1179680 | tf_op jit(solution)/shard_map/ppermute | solution.py:313
  213.2 18.9 %experts.5 = (f32[192,4096]{1,0:T(8,128)}, bf16[144,4096]{1,0:T(8,128)(2,1)S(1)}) custom-call(bf16[192,4096]{1,0:T(8,128)(2,1)S(1)} %copy-done.2, bf16[144,4096]{1,0:T(8,128)(2,1)} %collective-permute-done.21.refs_1_, f32[4,192]{1,0:T(4,128)S(1)} %get-tuple-element.53.refs_2_, f32[4,192]{1,0:T(4,128)S(1)} %get-tuple-element.52.refs_3_, ...), custom_call_target="tpu_custom_call" | custom-call | flops 3623878656 | bytes 37748736 | tf_op jit(solution)/shard_map/experts/pallas_call | solution.py:251
  234.9 26.0 %collective-permute-done.22.refs_1_ = bf16[144,4096]{1,0:T(8,128)(2,1)S(1)} collective-permute-done((bf16[144,4096]{1,0:T(8,128)(2,1)S(1)}, bf16[144,4096]{1,0:T(8,128)(2,1)S(1)}, u32[]{:S(2)}, u32[]{:S(2)}) %collective-permute-start.22) | collective-permute-done | bytes 1179680 | tf_op jit(solution)/shard_map/ppermute | solution.py:313
  270.6 10.9 %collective-permute-done.26.refs_1_ = bf16[144,4096]{1,0:T(8,128)(2,1)S(1)} collective-permute-done((bf16[144,4096]{1,0:T(8,128)(2,1)S(1)}, bf16[144,4096]{1,0:T(8,128)(2,1)S(1)}, u32[]{:S(2)}, u32[]{:S(2)}) %collective-permute-start.26) | collective-permute-done | bytes 1179680 | tf_op jit(solution)/shard_map/ppermute | solution.py:313
  281.5 18.1 %experts.7 = (f32[192,4096]{1,0:T(8,128)}, bf16[144,4096]{1,0:T(8,128)(2,1)}) custom-call(bf16[192,4096]{1,0:T(8,128)(2,1)S(1)} %add.313.refs_0_, bf16[144,4096]{1,0:T(8,128)(2,1)S(1)} %collective-permute-done.26.refs_1_, f32[4,192]{1,0:T(4,128)S(1)} %get-tuple-element.51.refs_2_, f32[4,192]{1,0:T(4,128)S(1)} %get-tuple-element.50.refs_3_, ...), custom_call_target="tpu_custom_call" | custom-call | flops 3623878656 | bytes 37748736 | tf_op jit(solution)/shard_map/experts/pallas_call | solution.py:251
  307.0 21.7 %collective-permute-done.27.refs_1_ = bf16[144,4096]{1,0:T(8,128)(2,1)} collective-permute-done((bf16[144,4096]{1,0:T(8,128)(2,1)}, bf16[144,4096]{1,0:T(8,128)(2,1)}, u32[]{:S(2)}, u32[]{:S(2)}) %collective-permute-start.27) | collective-permute-done | bytes 1179680 | tf_op jit(solution)/shard_map/ppermute | solution.py:313
  328.7 3.1 combine.7
  331.9 3.4 add_add_fusion
  339.6 8.6 %collective-permute-done.23.refs_1_ = bf16[144,4096]{1,0:T(8,128)(2,1)S(1)} collective-permute-done((bf16[144,4096]{1,0:T(8,128)(2,1)S(1)}, bf16[144,4096]{1,0:T(8,128)(2,1)S(1)}, u32[]{:S(2)}, u32[]{:S(2)}) %collective-permute-start.23) | collective-permute-done | bytes 1179680 | tf_op jit(solution)/shard_map/ppermute | solution.py:313
  348.2 18.2 %experts.6 = (f32[192,4096]{1,0:T(8,128)}, bf16[144,4096]{1,0:T(8,128)(2,1)}) custom-call(bf16[192,4096]{1,0:T(8,128)(2,1)S(1)} %copy-done.7, bf16[144,4096]{1,0:T(8,128)(2,1)S(1)} %collective-permute-done.23.refs_1_, f32[4,192]{1,0:T(4,128)S(1)} %get-tuple-element.49.refs_2_, f32[4,192]{1,0:T(4,128)S(1)} %get-tuple-element.48.refs_3_, ...), custom_call_target="tpu_custom_call" | custom-call | flops 3623878656 | bytes 37748736 | tf_op jit(solution)/shard_map/experts/pallas_call | solution.py:251
  374.7 20.8 %collective-permute-done.24.refs_1_ = bf16[144,4096]{1,0:T(8,128)(2,1)} collective-permute-done((bf16[144,4096]{1,0:T(8,128)(2,1)}, bf16[144,4096]{1,0:T(8,128)(2,1)}, u32[]{:S(2)}, u32[]{:S(2)}) %collective-permute-start.24) | collective-permute-done | bytes 1179680 | tf_op jit(solution)/shard_map/ppermute | solution.py:313
  397.4 3.1 combine.6
  400.6 3.0 select_add_fusion.1
  404.9 5.7 %collective-permute-start.31 = (bf16[192,4096]{1,0:T(8,128)(2,1)S(1)}, bf16[192,4096]{1,0:T(8,128)(2,1)}, u32[]{:S(2)}, u32[]{:S(2)}) collective-permute-start(bf16[192,4096]{1,0:T(8,128)(2,1)S(1)} %get-tuple-element.35), channel_id=1, source_target_pairs={{0,8},{4,12},{8,16},{12,20},{16,24},{20,28},{1,9},{5,13},{9,17},{1... | collective-permute-start | bytes 4718600 | tf_op jit(solution)/shard_map/ppermute | solution.py:305
  410.7 9.9 %collective-permute-done.5.refs_2_ = bf16[144,1024]{1,0:T(8,128)(2,1)S(1)} collective-permute-done((bf16[144,1024]{1,0:T(8,128)(2,1)S(1)}, bf16[144,1024]{1,0:T(8,128)(2,1)S(1)}, u32[]{:S(2)}, u32[]{:S(2)}) %collective-permute-start.5) | collective-permute-done | bytes 294944 | tf_op jit(solution)/shard_map/ppermute | solution.py:313
  420.5 9.0 %out_norm.2 = (bf16[192,4096]{1,0:T(8,128)(2,1)S(1)}, bf16[144,4096]{1,0:T(8,128)(2,1)S(1)}, bf16[192,4096]{1,0:T(8,128)(2,1)S(1)}) custom-call(s32[1]{0:T(128)} %bitcast.refs_0_, bf16[192,1024]{1,0:T(8,128)(2,1)S(1)} %pad_maximum_fusion.refs_1_, bf16[144,1024]{1,0:T(8,128)(2,1)S(1)} %collective-permute-done.5.refs_2_, bf16[192,4096]{1,0:T(8,128)(2,1)S(1)} %copy-done.9, ...), custom_call_target="tpu_custom_call" | custom-call | flops 2818572288 | bytes 5505024 | tf_op jit(solution)/shard_map/out_norm/pallas_call | solution.py:138
  430.8 18.3 %experts.4 = (f32[192,4096]{1,0:T(8,128)}, bf16[144,4096]{1,0:T(8,128)(2,1)S(1)}) custom-call(bf16[192,4096]{1,0:T(8,128)(2,1)S(1)} %get-tuple-element.21.refs_0_, bf16[144,4096]{1,0:T(8,128)(2,1)S(1)} %get-tuple-element.22.refs_1_, f32[4,192]{1,0:T(4,128)S(1)} %get-tuple-element.55.refs_2_, f32[4,192]{1,0:T(4,128)S(1)} %get-tuple-element.54.refs_3_, ...), custom_call_target="tpu_custom_call" | custom-call | flops 3623878656 | bytes 37748736 | tf_op jit(solution)/shard_map/experts/pallas_call | solution.py:251
  451.8 18.8 %collective-permute-done.10.refs_1_ = bf16[144,4096]{1,0:T(8,128)(2,1)S(1)} collective-permute-done((bf16[144,4096]{1,0:T(8,128)(2,1)S(1)}, bf16[144,4096]{1,0:T(8,128)(2,1)S(1)}, u32[]{:S(2)}, u32[]{:S(2)}) %collective-permute-start.10) | collective-permute-done | bytes 1179680 | tf_op jit(solution)/shard_map/ppermute | solution.py:313
  473.4 7.7 %add_convert_fusion = bf16[192,4096]{1,0:T(8,128)(2,1)} fusion(bf16[192,4096]{1,0:T(8,128)(2,1)} %collective-permute-done.33, bf16[192,4096]{1,0:T(8,128)(2,1)} %collective-permute-done.31, bf16[192,4096]{1,0:T(8,128)(2,1)} %copy-done.10, bf16[192,4096]{1,0:T(8,128)(2,1)} %copy-done.16, bf16[384,4096]{1,0:T(8,128)(2,1)S(1)} %copy-done, ...), kind=kOutput, calls=%fused_computation.4 | convolution fusion | flops 1215479808 | bytes 16023552 | tf_op jit(solution)/shard_map/dot_general | solution.py:447
  (180 shorter events, 91.8 us)
Async XLA Ops:
  0.0 48.9 %collective-permute-start.8 = (bf16[256,4096]{1,0:T(8,128)(2,1)}, bf16[256,4096]{1,0:T(8,128)(2,1)}, u32[]{:S(2)}, u32[]{:S(2)}) collective-permute-start(bf16[256,4096]{1,0:T(8,128)(2,1)} %refs_6_.8), channel_id=1, source_target_pairs={{0,2},{1,3},{2,0},{3,1},{4,6},{5,7},{6,4},{7,5},{8,10},{9,11},{10,... | collective-permute-start | bytes 6291464 | tf_op jit(solution)/shard_map/ppermute | solution.py:316
  3.0 86.1 %collective-permute-start.13 = (bf16[192,4096]{1,0:T(8,128)(2,1)}, bf16[192,4096]{1,0:T(8,128)(2,1)}, u32[]{:S(2)}, u32[]{:S(2)}) collective-permute-start(bf16[192,4096]{1,0:T(8,128)(2,1)} %refs_3_.1), channel_id=1, source_target_pairs={{0,8},{4,12},{8,16},{12,20},{16,24},{20,28},{1,9},{5,13},{9,17},{1... | collective-permute-start | bytes 4718600 | tf_op jit(solution)/shard_map/ppermute | solution.py:305
  7.7 81.3 %collective-permute-start.14 = (bf16[192,4096]{1,0:T(8,128)(2,1)}, bf16[192,4096]{1,0:T(8,128)(2,1)}, u32[]{:S(2)}, u32[]{:S(2)}) collective-permute-start(bf16[192,4096]{1,0:T(8,128)(2,1)} %refs_3_.1), channel_id=1, source_target_pairs={{24,16},{28,20},{16,8},{20,12},{8,0},{12,4},{25,17},{29,21},{17,9}... | collective-permute-start | bytes 4718600 | tf_op jit(solution)/shard_map/ppermute | solution.py:305
  9.7 5.9 %collective-permute-start.1 = (bf16[8,256]{1,0:T(8,128)(2,1)S(1)}, bf16[8,256]{1,0:T(8,128)(2,1)S(1)}, u32[]{:S(2)}, u32[]{:S(2)}) collective-permute-start(bf16[8,256]{1,0:T(8,128)(2,1)S(1)} %get-tuple-element.42), channel_id=1, source_target_pairs={{4,0},{8,4},{12,8},{16,12},{20,16},{24,20},{28,24},{5,1},{9,5},{13... | collective-permute-start | bytes 12296 | tf_op jit(solution)/shard_map/ppermute | solution.py:29
  11.0 5.9 %collective-permute-start = (bf16[8,256]{1,0:T(8,128)(2,1)S(1)}, bf16[8,256]{1,0:T(8,128)(2,1)S(1)}, u32[]{:S(2)}, u32[]{:S(2)}) collective-permute-start(bf16[8,256]{1,0:T(8,128)(2,1)S(1)} %get-tuple-element.41), channel_id=1, source_target_pairs={{0,4},{4,8},{8,12},{12,16},{16,20},{20,24},{24,28},{1,5},{5,9},{9,... | collective-permute-start | bytes 12296 | tf_op jit(solution)/shard_map/ppermute | solution.py:27
  15.6 73.4 %collective-permute-start.7 = (bf16[256,4096]{1,0:T(8,128)(2,1)}, bf16[256,4096]{1,0:T(8,128)(2,1)}, u32[]{:S(2)}, u32[]{:S(2)}) collective-permute-start(bf16[256,4096]{1,0:T(8,128)(2,1)} %refs_6_.8), channel_id=1, source_target_pairs={{0,1},{1,0},{2,3},{3,2},{4,5},{5,4},{6,7},{7,6},{8,9},{9,8},{10,11... | collective-permute-start | bytes 6291464 | tf_op jit(solution)/shard_map/ppermute | solution.py:316
  48.9 40.1 %collective-permute-start.9 = (bf16[256,4096]{1,0:T(8,128)(2,1)}, bf16[256,4096]{1,0:T(8,128)(2,1)}, u32[]{:S(2)}, u32[]{:S(2)}) collective-permute-start(bf16[256,4096]{1,0:T(8,128)(2,1)} %collective-permute-done.8.refs_8_), channel_id=1, source_target_pairs={{0,1},{1,0},{2,3},{3,2},{4,5},{5,4},{6,7},{7,6},{8,9},{9,8},{10,11... | collective-permute-start | bytes 6291464 | tf_op jit(solution)/shard_map/ppermute | solution.py:316
  56.5 5.1 %collective-permute-start.3 = (bf16[192,256]{1,0:T(8,128)(2,1)S(1)}, bf16[192,256]{1,0:T(8,128)(2,1)S(1)}, u32[]{:S(2)}, u32[]{:S(2)}) collective-permute-start(bf16[192,256]{1,0:T(8,128)(2,1)S(1)} %get-tuple-element.39), channel_id=1, source_target_pairs={{0,2},{1,3},{2,0},{3,1},{4,6},{5,7},{6,4},{7,5},{8,10},{9,11},{10,... | collective-permute-start | bytes 294920 | tf_op jit(solution)/shard_map/ppermute | solution.py:316
  62.9 12.3 %collective-permute-start.11 = (bf16[192,1024]{1,0:T(8,128)(2,1)S(1)}, bf16[192,1024]{1,0:T(8,128)(2,1)S(1)}, u32[]{:S(2)}, u32[]{:S(2)}) collective-permute-start(bf16[192,1024]{1,0:T(8,128)(2,1)S(1)} %pad_maximum_fusion.refs_1_), channel_id=1, source_target_pairs={{0,8},{4,12},{8,16},{12,20},{16,24},{20,28},{1,9},{5,13},{9,17},{1... | collective-permute-start | bytes 1179656 | tf_op jit(solution)/shard_map/ppermute | solution.py:305
  76.0 13.1 %collective-permute-start.12 = (bf16[192,1024]{1,0:T(8,128)(2,1)S(1)}, bf16[192,1024]{1,0:T(8,128)(2,1)}, u32[]{:S(2)}, u32[]{:S(2)}) collective-permute-start(bf16[192,1024]{1,0:T(8,128)(2,1)S(1)} %pad_maximum_fusion.refs_1_), channel_id=1, source_target_pairs={{24,16},{28,20},{16,8},{20,12},{8,0},{12,4},{25,17},{29,21},{17,9}... | collective-permute-start | bytes 1179656 | tf_op jit(solution)/shard_map/ppermute | solution.py:305
  106.2 37.2 %collective-permute-start.17 = (bf16[192,4096]{1,0:T(8,128)(2,1)}, bf16[192,4096]{1,0:T(8,128)(2,1)}, u32[]{:S(2)}, u32[]{:S(2)}) collective-permute-start(bf16[192,4096]{1,0:T(8,128)(2,1)} %get-tuple-element.27), channel_id=1, source_target_pairs={{16,8},{20,12},{8,0},{12,4},{17,9},{21,13},{9,1},{13,5},{18,10},{2... | collective-permute-start | bytes 4718600 | tf_op jit(solution)/shard_map/ppermute | solution.py:305
  107.5 37.2 %collective-permute-start.15 = (bf16[192,4096]{1,0:T(8,128)(2,1)}, bf16[192,4096]{1,0:T(8,128)(2,1)}, u32[]{:S(2)}, u32[]{:S(2)}) collective-permute-start(bf16[192,4096]{1,0:T(8,128)(2,1)} %get-tuple-element.26), channel_id=1, source_target_pairs={{8,16},{12,20},{16,24},{20,28},{9,17},{13,21},{17,25},{21,29},{10,... | collective-permute-start | bytes 4718600 | tf_op jit(solution)/shard_map/ppermute | solution.py:305
  143.5 39.3 %collective-permute-start.18 = (bf16[192,4096]{1,0:T(8,128)(2,1)}, bf16[192,4096]{1,0:T(8,128)(2,1)}, u32[]{:S(2)}, u32[]{:S(2)}) collective-permute-start(bf16[192,4096]{1,0:T(8,128)(2,1)} %collective-permute-done.17), channel_id=1, source_target_pairs={{8,0},{12,4},{9,1},{13,5},{10,2},{14,6},{11,3},{15,7}} | collective-permute-start | bytes 4718600 | tf_op jit(solution)/shard_map/ppermute | solution.py:305
  144.8 38.0 %collective-permute-start.16 = (bf16[192,4096]{1,0:T(8,128)(2,1)}, bf16[192,4096]{1,0:T(8,128)(2,1)}, u32[]{:S(2)}, u32[]{:S(2)}) collective-permute-start(bf16[192,4096]{1,0:T(8,128)(2,1)} %collective-permute-done.15), channel_id=1, source_target_pairs={{16,24},{20,28},{17,25},{21,29},{18,26},{22,30},{19,27},{23,31}} | collective-permute-start | bytes 4718600 | tf_op jit(solution)/shard_map/ppermute | solution.py:305
  148.9 31.7 %collective-permute-start.20 = (f32[2,8,192]{2,1,0:T(8,128)}, f32[2,8,192]{2,1,0:T(8,128)}, u32[]{:S(2)}, u32[]{:S(2)}) collective-permute-start(f32[2,8,192]{2,1,0:T(8,128)} %get-tuple-element.45), channel_id=1, source_target_pairs={{0,24},{4,28},{8,0},{12,4},{16,8},{20,12},{24,16},{28,20},{1,25},{... | collective-permute-start | bytes 36872 | tf_op jit(solution)/shard_map/ppermute | solution.py:305
  152.5 28.0 %collective-permute-start.19 = (f32[2,8,192]{2,1,0:T(8,128)}, f32[2,8,192]{2,1,0:T(8,128)}, u32[]{:S(2)}, u32[]{:S(2)}) collective-permute-start(f32[2,8,192]{2,1,0:T(8,128)} %get-tuple-element.44), channel_id=1, source_target_pairs={{0,8},{4,12},{8,16},{12,20},{16,24},{20,28},{24,0},{28,4},{1,9},{5... | collective-permute-start | bytes 36872 | tf_op jit(solution)/shard_map/ppermute | solution.py:305
  188.0 25.2 %collective-permute-start.21 = (bf16[144,4096]{1,0:T(8,128)(2,1)}, bf16[144,4096]{1,0:T(8,128)(2,1)}, u32[]{:S(2)}, u32[]{:S(2)}) collective-permute-start(bf16[144,4096]{1,0:T(8,128)(2,1)} %convolution_convert_fusion.2), channel_id=1, source_target_pairs={{0,4},{4,0},{8,12},{12,8},{16,20},{20,16},{24,28},{28,24},{1,5},{5... | collective-permute-start | bytes 3538952 | tf_op jit(solution)/shard_map/ppermute | solution.py:313
  189.5 5.1 %collective-permute-start.25 = (f32[2,8,192]{2,1,0:T(8,128)}, f32[2,8,192]{2,1,0:T(8,128)}, u32[]{:S(2)}, u32[]{:S(2)}) collective-permute-start(f32[2,8,192]{2,1,0:T(8,128)} %get-tuple-element.43), channel_id=1, source_target_pairs={{0,16},{4,20},{8,24},{12,28},{16,0},{20,4},{24,8},{28,12},{1,17},{... | collective-permute-start | bytes 36872 | tf_op jit(solution)/shard_map/ppermute | solution.py:305
  232.1 28.9 %collective-permute-start.22 = (bf16[144,4096]{1,0:T(8,128)(2,1)S(1)}, bf16[144,4096]{1,0:T(8,128)(2,1)S(1)}, u32[]{:S(2)}, u32[]{:S(2)}) collective-permute-start(bf16[144,4096]{1,0:T(8,128)(2,1)S(1)} %get-tuple-element.29), channel_id=1, source_target_pairs={{0,4},{4,0},{8,12},{12,8},{16,20},{20,16},{24,28},{28,24},{1,5},{5... | collective-permute-start | bytes 3538952 | tf_op jit(solution)/shard_map/ppermute | solution.py:313
  234.2 47.3 %collective-permute-start.26 = (bf16[144,4096]{1,0:T(8,128)(2,1)S(1)}, bf16[144,4096]{1,0:T(8,128)(2,1)S(1)}, u32[]{:S(2)}, u32[]{:S(2)}) collective-permute-start(bf16[144,4096]{1,0:T(8,128)(2,1)S(1)} %convolution_convert_fusion), channel_id=1, source_target_pairs={{0,4},{4,0},{8,12},{12,8},{16,20},{20,16},{24,28},{28,24},{1,5},{5... | collective-permute-start | bytes 3538952 | tf_op jit(solution)/shard_map/ppermute | solution.py:313
  265.5 66.3 %collective-permute-start.29 = (bf16[192,4096]{1,0:T(8,128)(2,1)}, bf16[192,4096]{1,0:T(8,128)(2,1)}, u32[]{:S(2)}, u32[]{:S(2)}) collective-permute-start(bf16[192,4096]{1,0:T(8,128)(2,1)} %combine.5), channel_id=1, source_target_pairs={{24,16},{28,20},{25,17},{29,21},{26,18},{30,22},{27,19},{31,23}} | collective-permute-start | bytes 4718600 | tf_op jit(solution)/shard_map/ppermute | solution.py:305
  267.3 64.5 %collective-permute-start.28 = (bf16[192,4096]{1,0:T(8,128)(2,1)}, bf16[192,4096]{1,0:T(8,128)(2,1)}, u32[]{:S(2)}, u32[]{:S(2)}) collective-permute-start(bf16[192,4096]{1,0:T(8,128)(2,1)} %combine.5), channel_id=1, source_target_pairs={{0,8},{4,12},{1,9},{5,13},{2,10},{6,14},{3,11},{7,15}} | collective-permute-start | bytes 4718600 | tf_op jit(solution)/shard_map/ppermute | solution.py:305
  299.6 29.2 %collective-permute-start.27 = (bf16[144,4096]{1,0:T(8,128)(2,1)}, bf16[144,4096]{1,0:T(8,128)(2,1)}, u32[]{:S(2)}, u32[]{:S(2)}) collective-permute-start(bf16[144,4096]{1,0:T(8,128)(2,1)} %get-tuple-element.34), channel_id=1, source_target_pairs={{0,4},{4,0},{8,12},{12,8},{16,20},{20,16},{24,28},{28,24},{1,5},{5... | collective-permute-start | bytes 3538952 | tf_op jit(solution)/shard_map/ppermute | solution.py:313
  306.5 41.7 %collective-permute-start.23 = (bf16[144,4096]{1,0:T(8,128)(2,1)S(1)}, bf16[144,4096]{1,0:T(8,128)(2,1)S(1)}, u32[]{:S(2)}, u32[]{:S(2)}) collective-permute-start(bf16[144,4096]{1,0:T(8,128)(2,1)S(1)} %convolution_convert_fusion.1), channel_id=1, source_target_pairs={{0,4},{4,0},{8,12},{12,8},{16,20},{20,16},{24,28},{28,24},{1,5},{5... | collective-permute-start | bytes 3538952 | tf_op jit(solution)/shard_map/ppermute | solution.py:313
  335.2 65.3 %collective-permute-start.30 = (bf16[192,4096]{1,0:T(8,128)(2,1)}, bf16[192,4096]{1,0:T(8,128)(2,1)}, u32[]{:S(2)}, u32[]{:S(2)}) collective-permute-start(bf16[192,4096]{1,0:T(8,128)(2,1)} %add_add_fusion), channel_id=1, source_target_pairs={{0,8},{4,12},{8,16},{12,20},{1,9},{5,13},{9,17},{13,21},{2,10},{6,... | collective-permute-start | bytes 4718600 | tf_op jit(solution)/shard_map/ppermute | solution.py:305
  337.8 62.8 %collective-permute-start.32 = (bf16[192,4096]{1,0:T(8,128)(2,1)}, bf16[192,4096]{1,0:T(8,128)(2,1)}, u32[]{:S(2)}, u32[]{:S(2)}) collective-permute-start(bf16[192,4096]{1,0:T(8,128)(2,1)} %add_add_fusion), channel_id=1, source_target_pairs={{24,16},{28,20},{16,8},{20,12},{25,17},{29,21},{17,9},{21,13},{26,... | collective-permute-start | bytes 4718600 | tf_op jit(solution)/shard_map/ppermute | solution.py:305
  366.4 29.2 %collective-permute-start.24 = (bf16[144,4096]{1,0:T(8,128)(2,1)}, bf16[144,4096]{1,0:T(8,128)(2,1)}, u32[]{:S(2)}, u32[]{:S(2)}) collective-permute-start(bf16[144,4096]{1,0:T(8,128)(2,1)} %get-tuple-element.32), channel_id=1, source_target_pairs={{0,4},{4,0},{8,12},{12,8},{16,20},{20,16},{24,28},{28,24},{1,5},{5... | collective-permute-start | bytes 3538952 | tf_op jit(solution)/shard_map/ppermute | solution.py:313
  369.6 50.9 %collective-permute-start.6 = (bf16[144,4096]{1,0:T(8,128)(2,1)}, bf16[144,4096]{1,0:T(8,128)(2,1)}, u32[]{:S(2)}, u32[]{:S(2)}) collective-permute-start(bf16[144,4096]{1,0:T(8,128)(2,1)} %convolution_convert_fusion.3), channel_id=1, source_target_pairs={{0,4},{4,0},{8,12},{12,8},{16,20},{20,16},{24,28},{28,24},{1,5},{5... | collective-permute-start | bytes 3538952 | tf_op jit(solution)/shard_map/ppermute | solution.py:313
  373.2 47.3 %collective-permute-start.5 = (bf16[144,1024]{1,0:T(8,128)(2,1)S(1)}, bf16[144,1024]{1,0:T(8,128)(2,1)S(1)}, u32[]{:S(2)}, u32[]{:S(2)}) collective-permute-start(bf16[144,1024]{1,0:T(8,128)(2,1)S(1)} %convolution_convert_fusion.4), channel_id=1, source_target_pairs={{0,4},{4,0},{8,12},{12,8},{16,20},{20,16},{24,28},{28,24},{1,5},{5... | collective-permute-start | bytes 884744 | tf_op jit(solution)/shard_map/ppermute | solution.py:313
  403.6 69.8 %collective-permute-start.33 = (bf16[192,4096]{1,0:T(8,128)(2,1)S(1)}, bf16[192,4096]{1,0:T(8,128)(2,1)}, u32[]{:S(2)}, u32[]{:S(2)}) collective-permute-start(bf16[192,4096]{1,0:T(8,128)(2,1)S(1)} %get-tuple-element.36), channel_id=1, source_target_pairs={{24,16},{28,20},{16,8},{20,12},{8,0},{12,4},{25,17},{29,21},{17,9}... | collective-permute-start | bytes 4718600 | tf_op jit(solution)/shard_map/ppermute | solution.py:305
  404.9 68.5 %collective-permute-start.31 = (bf16[192,4096]{1,0:T(8,128)(2,1)S(1)}, bf16[192,4096]{1,0:T(8,128)(2,1)}, u32[]{:S(2)}, u32[]{:S(2)}) collective-permute-start(bf16[192,4096]{1,0:T(8,128)(2,1)S(1)} %get-tuple-element.35), channel_id=1, source_target_pairs={{0,8},{4,12},{8,16},{12,20},{16,24},{20,28},{1,9},{5,13},{9,17},{1... | collective-permute-start | bytes 4718600 | tf_op jit(solution)/shard_map/ppermute | solution.py:305
  449.1 21.6 %collective-permute-start.10 = (bf16[144,4096]{1,0:T(8,128)(2,1)S(1)}, bf16[144,4096]{1,0:T(8,128)(2,1)S(1)}, u32[]{:S(2)}, u32[]{:S(2)}) collective-permute-start(bf16[144,4096]{1,0:T(8,128)(2,1)S(1)} %get-tuple-element.24), channel_id=1, source_target_pairs={{0,4},{4,0},{8,12},{12,8},{16,20},{20,16},{24,28},{28,24},{1,5},{5... | collective-permute-start | bytes 3538952 | tf_op jit(solution)/shard_map/ppermute | solution.py:313
  (47 other events, 1032.5 us)
where the time goes:
time: 483 us; the launch traced here: 481 us
  waiting for transfers between devices  253 us (52%)
  Pallas kernels  105 us (22%)
  starting transfers between devices  62.9 us (13%)
  matrix products  23.7 us (5%)
  local copies, waits for them, and re-layouts  19 us (4%)
  other arithmetic  17.1 us (4%)
    ppermute x9, waiting for transfers between devices, along_inner(): return lax.ppermute(x, 'sp', pairs)  130 us
    ppermute x17, waiting for transfers between devices, along_outer(): return lax.ppermute(x, 'sp', pairs)  82.5 us
    pallas_call x4, Pallas kernels, run_experts(): pl.pallas_call(functools.partial(expert_kernel, peers, capacity, pad), gr...  73.4 us
    ppermute x17, starting transfers between devices, along_outer(): return lax.ppermute(x, 'sp', pairs)  39.8 us
    ppermute x6, waiting for transfers between devices, along_tp(): return lax.ppermute(x, 'tp', [(i, i ^ bits) for i in range(n_tp)])  38.7 us
    pallas_call x2, Pallas kernels, out_norm(): pl.pallas_call(functools.partial(out_norm_kernel, blocks, keep, pick), ou...  21.3 us
    unnamed x90, local copies, waits for them, and re-layouts  13.6 us
    ppermute x9, starting transfers between devices, along_inner(): return lax.ppermute(x, 'sp', pairs)  10.9 us
  transfers between devices with their start and end apart: 34, of which 18 were waited for; matrix products, arithmetic and copies ran while one was open for 7% of the time, Pallas kernels for 15%

commit v1 on v0

--- a/solution.py
+++ b/solution.py
@@ -67,13 +67,17 @@
     return (mixed_rows.reshape(tok_local, -1) * pool_scale[None, :]).astype(bf16)
 
 
-def out_norm_kernel(blocks, keep, pick, *refs):
-    plane, refs = refs[0], refs[1:]
+def out_norm_kernel(blocks, keep, halved, *refs):
     pools, resids = refs[:blocks], refs[blocks : 2 * blocks]
     refs = refs[2 * blocks :]
-    gain, weights, outs = refs[0], refs[1:5], refs[5:]
+    gain, refs = refs[0], refs[1:]
+    weights = []
+    for parts in halved:
+        weights.append(refs[:parts])
+        refs = refs[parts:]
+    outs = refs
     width = gain.shape[1]
-    depth = weights[0].shape[0]
+    depth = weights[0][0].shape[0]
     step = 1024
     steps = width // step
 
@@ -85,70 +89,52 @@
         normed = outs[i]
         middle = outs[blocks] if keep and i == 0 else normed
 
-        def project(n, total):
-            at = part(n)
+        def project(half, n, total):
+            at = part(n + half * (steps // 2))
             acc = resid[:, at].astype(f32)
             for j, weight in enumerate(weights):
+                rows = weight[half][:, part(n)] if len(weight) == 2 else weight[0][:, at]
                 acc = acc + jnp.dot(
-                    pool[:, j * depth : (j + 1) * depth],
-                    weight[:, at],
-                    preferred_element_type=f32,
+                    pool[:, j * depth : (j + 1) * depth], rows, preferred_element_type=f32
                 )
             mid = acc.astype(bf16)
             middle[:, at] = mid
             mid = mid.astype(f32)
             return total + jnp.sum(mid * mid, axis=1, keepdims=True)
 
-        total = lax.fori_loop(0, steps, project, jnp.zeros((resid.shape[0], 1), f32))
+        total = jnp.zeros((resid.shape[0], 1), f32)
+        for half in range(2):
+            total = lax.fori_loop(0, steps // 2, functools.partial(project, half), total)
         scale = lax.rsqrt(total * (1.0 / width) + norm_eps)
 
         def finish(n, carry):
             at = part(n)
-            value = (middle[:, at].astype(f32) * scale * gain[:, at]).astype(bf16)
-            normed[:, at] = value
-            if pick:
-                near, spare = outs[blocks], outs[blocks + 1]
-                low = plane[0] <= 1
-
-                @pl.when(low if i == 1 else jnp.logical_not(low))
-                def _():
-                    near[:, at] = value
-
-                @pl.when(plane[0] == 1 + i)
-                def _():
-                    spare[:, at] = value
-
-                if i == 0:
-
-                    @pl.when((plane[0] != 1) & (plane[0] != 2))
-                    def _():
-                        spare[:, at] = jnp.zeros_like(value)
-
+            normed[:, at] = (middle[:, at].astype(f32) * scale * gain[:, at]).astype(bf16)
             return carry
 
         lax.fori_loop(0, steps, finish, 0)
 
 
-def out_norm(pools, resids, gain, weights, plane, keep, pick):
+def out_norm(pools, resids, gain, weights, keep):
     blocks = len(pools)
     vm = pl.BlockSpec(memory_space=pltpu.VMEM)
     shapes = [jax.ShapeDtypeStruct(r.shape, bf16) for r in resids]
-    shapes += [shapes[0]] * (1 if keep else 2 if pick else 0)
+    shapes += [shapes[0]] * (1 if keep else 0)
     rows = sum(r.shape[0] for r in resids)
+    flat = [w for group in weights for w in group]
     return pl.pallas_call(
-        functools.partial(out_norm_kernel, blocks, keep, pick),
+        functools.partial(out_norm_kernel, blocks, keep, [len(g) for g in weights]),
         out_shape=shapes,
-        in_specs=[pl.BlockSpec(memory_space=pltpu.SMEM)]
-        + [vm] * (2 * blocks + 1 + len(weights)),
+        in_specs=[vm] * (2 * blocks + 1 + len(flat)),
         out_specs=[vm] * len(shapes),
-        compiler_params=pltpu.CompilerParams(vmem_limit_bytes=40 * 2**20),
+        compiler_params=pltpu.CompilerParams(vmem_limit_bytes=36 * 2**20),
         cost_estimate=pl.CostEstimate(
             flops=2 * rows * pools[0].shape[1] * gain.shape[0],
             bytes_accessed=4 * rows * gain.shape[0],
             transcendentals=rows,
         ),
         name="out_norm",
-    )(plane.reshape(1), *pools, *resids, gain.reshape(1, -1), *weights)
+    )(*pools, *resids, gain.reshape(1, -1), *flat)
 
 
 def combine_kernel(count, own, *refs):
@@ -161,39 +147,68 @@
     out[...] = total.astype(bf16)
 
 
-def combine(own, mixes, parts):
+def combine(own, mixes, parts, half):
     count = len(parts)
     rows, width = own.shape
     step = width // 4
+    skip = 2 * half
+    cut_parts = parts[0].shape[1] == width
     whole = [pl.BlockSpec(m.shape, lambda n: (0, 0)) for m in mixes]
-    cut = [pl.BlockSpec((p.shape[0], step), lambda n: (0, n)) for p in parts]
-    mine = pl.BlockSpec((rows, step), lambda n: (0, n))
+    cut = [
+        pl.BlockSpec((p.shape[0], step), lambda n: (0, n + (skip if cut_parts else 0)))
+        for p in parts
+    ]
     return pl.pallas_call(
         functools.partial(combine_kernel, count),
-        grid=(4,),
-        out_shape=jax.ShapeDtypeStruct(own.shape, bf16),
-        in_specs=[mine] + whole + cut,
-        out_specs=mine,
+        grid=(2,),
+        out_shape=jax.ShapeDtypeStruct((rows, width // 2), bf16),
+        in_specs=[pl.BlockSpec((rows, step), lambda n: (0, n + skip))] + whole + cut,
+        out_specs=pl.BlockSpec((rows, step), lambda n: (0, n)),
         compiler_params=pltpu.CompilerParams(vmem_limit_bytes=24 * 2**20),
         cost_estimate=pl.CostEstimate(
-            flops=2 * rows * width * sum(p.shape[0] for p in parts),
-            bytes_accessed=8 * rows * width,
+            flops=rows * width * sum(p.shape[0] for p in parts),
+            bytes_accessed=4 * rows * width,
             transcendentals=0,
         ),
         name="combine",
     )(own, *mixes, *parts)
 
 
-def expert_kernel(peers, capacity, pad, *refs):
-    line, others, refs = refs[0], refs[1 : 1 + peers], refs[1 + peers :]
+def finish_kernel(base, own_a, own_b, up_a, up_b, down_a, down_b, out):
+    span = own_a.shape[1]
+    for h, group in enumerate(((own_a, up_a, down_a), (own_b, up_b, down_b))):
+        at = slice(h * span, (h + 1) * span)
+        total = base[:, at]
+        for part in group:
+            total = total + part[...].astype(f32)
+        out[:, at] = total.astype(bf16)
+
+
+def finish(base, *parts):
+    vm = pl.BlockSpec(memory_space=pltpu.VMEM)
+    return pl.pallas_call(
+        finish_kernel,
+        out_shape=jax.ShapeDtypeStruct(base.shape, bf16),
+        in_specs=[vm] * (1 + len(parts)),
+        out_specs=vm,
+        compiler_params=pltpu.CompilerParams(vmem_limit_bytes=20 * 2**20),
+        name="finish",
+    )(base, *parts)
+
+
+def expert_kernel(peers, parts, capacity, pad, *refs):
+    line, refs = refs[:parts], refs[parts:]
+    others = [refs[j * parts : (j + 1) * parts] for j in range(peers)]
+    refs = refs[peers * parts :]
     rank, share, gate, up, down, own = refs[:6]
-    backs = refs[6 : 6 + peers]
-    packed, made, pick, mixing, shift = refs[6 + peers :]
+    backs = [refs[6 + j * parts : 6 + (j + 1) * parts] for j in range(peers)]
+    packed, made, pick, mixing, shift = refs[6 + peers * parts :]
     expert = pl.program_id(0)
     count = pl.num_programs(0)
     experts = rank.shape[0]
-    rows = line.shape[0]
-    other_rows = others[0].shape[0]
+    rows, span = line[0].shape
+    other_rows = others[0][0].shape[0]
+    step = 1024
 
     @pl.when(expert == 0)
     def _():
@@ -209,57 +224,95 @@
             shift[here, :] = (
                 ((col == e * capacity + row) & (row < capacity)).astype(f32).astype(bf16)
             )
+        for h in range(parts):
+
+            def gather(n, carry):
+                at = pl.ds(pl.multiple_of(n * step, step), step)
+                to = pl.ds(pl.multiple_of(h * span + n * step, step), step)
+                for i in range(1 + peers):
+                    source, chooser = (line, pick) if i == 0 else (others[i - 1], shift)
+                    moved = jnp.dot(
+                        chooser[...], source[h][:, at], preferred_element_type=f32
+                    ).astype(bf16)
+                    for e in range(experts):
+                        packed[e, i * pad : (i + 1) * pad, to] = moved[e * pad : (e + 1) * pad]
+                return carry
+
+            lax.fori_loop(0, span // step, gather, 0)
+
+    width = packed.shape[2]
+    wide = gate.shape[2]
+    filled = packed.shape[1]
+
+    def project(n, carry):
+        at = pl.ds(pl.multiple_of(n * step, step), step)
+        tokens = packed[expert, :, at]
+        return (
+            carry[0] + jnp.dot(tokens, gate[0, at, :], preferred_element_type=f32),
+            carry[1] + jnp.dot(tokens, up[0, at, :], preferred_element_type=f32),
+        )
+
+    zero = jnp.zeros((filled, wide), f32)
+    gated, lifted = lax.fori_loop(0, width // step, project, (zero, zero))
+    hidden = (gated * (1.0 / (1.0 + jnp.exp(-gated))) * lifted).astype(bf16)
+
+    def lower(n, carry):
+        at = pl.ds(pl.multiple_of(n * step, step), step)
+        result = jnp.dot(hidden, down[0, :, at], preferred_element_type=f32).astype(bf16)
         for i in range(1 + peers):
-            if i == 0:
-                moved = jnp.dot(pick[...], line[...], preferred_element_type=f32)
-            else:
-                moved = jnp.dot(shift[...], others[i - 1][...], preferred_element_type=f32)
-            moved = moved.astype(bf16)
-            for e in range(experts):
-                packed[e, i * pad : (i + 1) * pad, :] = moved[e * pad : (e + 1) * pad]
-
-    tokens = packed[expert]
-    gated = jnp.dot(tokens, gate[0], preferred_element_type=f32)
-    lifted = jnp.dot(tokens, up[0], preferred_element_type=f32)
-    hidden = (gated * (1.0 / (1.0 + jnp.exp(-gated))) * lifted).astype(bf16)
-    result = jnp.dot(hidden, down[0], preferred_element_type=f32).astype(bf16)
-    for i in range(1 + peers):
-        made[i, pl.ds(pl.multiple_of(expert * pad, pad), pad), :] = result[i * pad : (i + 1) * pad]
+            made[i, pl.ds(pl.multiple_of(expert * pad, pad), pad), at] = result[
+                i * pad : (i + 1) * pad
+            ]
+        return carry
+
+    lax.fori_loop(0, width // step, lower, 0)
 
     @pl.when(expert == count - 1)
     def _():
         rows_in = (((0,), (0,)), ((), ()))
-        own[...] = lax.dot_general(mixing[...], made[0], rows_in, preferred_element_type=f32)
-        for j in range(peers):
-            backs[j][...] = lax.dot_general(
-                shift[...], made[1 + j], rows_in, preferred_element_type=f32
-            ).astype(bf16)
+        for h in range(parts):
+
+            def spread(n, carry):
+                at = pl.ds(pl.multiple_of(n * step, step), step)
+                come = pl.ds(pl.multiple_of(h * span + n * step, step), step)
+                own[:, come] = lax.dot_general(
+                    mixing[...], made[0, :, come], rows_in, preferred_element_type=f32
+                )
+                for j in range(peers):
+                    backs[j][h][:, at] = lax.dot_general(
+                        shift[...], made[1 + j, :, come], rows_in, preferred_element_type=f32
+                    ).astype(bf16)
+                return carry
+
+            lax.fori_loop(0, span // step, spread, 0)
 
 
 def run_experts(line, others, rank, share, gate, up, down, capacity):
     peers = len(others)
+    parts = len(line)
     experts, width, hidden = gate.shape
     pad = -(-capacity // 16) * 16
-    rows = line.shape[0]
+    rows = line[0].shape[0]
     vm = pl.BlockSpec(memory_space=pltpu.VMEM)
+    flat = [h for group in others for h in group]
 
     def per_expert(a):
         return pl.BlockSpec((1,) + a.shape[1:], lambda e: (e, 0, 0))
 
-    back_shape = jax.ShapeDtypeStruct(others[0].shape, bf16)
+    back_shape = jax.ShapeDtypeStruct(flat[0].shape, bf16)
     filled = (1 + peers) * pad
     outs = pl.pallas_call(
-        functools.partial(expert_kernel, peers, capacity, pad),
+        functools.partial(expert_kernel, peers, parts, capacity, pad),
         grid=(experts,),
-        out_shape=[jax.ShapeDtypeStruct(line.shape, f32)] + [back_shape] * peers,
-        in_specs=[vm] * (3 + peers) + [per_expert(a) for a in (gate, up, down)],
-        out_specs=[vm] * (1 + peers),
+        out_shape=[jax.ShapeDtypeStruct((rows, width), f32)] + [back_shape] * len(flat),
+        in_specs=[vm] * (parts + len(flat) + 2) + [per_expert(a) for a in (gate, up, down)],
+        out_specs=[vm] * (1 + len(flat)),
         scratch_shapes=[
             pltpu.VMEM((experts, filled, width), bf16),
             pltpu.VMEM((1 + peers, experts * pad, width), bf16),
             pltpu.VMEM((experts * pad, rows), bf16),
             pltpu.VMEM((experts * pad, rows), bf16),
-            pltpu.VMEM((experts * pad, others[0].shape[0]), bf16),
+            pltpu.VMEM((experts * pad, flat[0].shape[0]), bf16),
         ],
         compiler_params=pltpu.CompilerParams(
             vmem_limit_bytes=48 * 2**20, dimension_semantics=("arbitrary",)
@@ -270,8 +323,8 @@
             transcendentals=experts * filled * hidden,
         ),
         name="experts",
-    )(line, *others, rank, share, gate, up, down)
-    return outs[0], outs[1:]
+    )(*line, *flat, rank, share, gate, up, down)
+    return outs[0], [outs[1 + j * parts : 1 + (j + 1) * parts] for j in range(peers)]
 
 
 def shards(
@@ -318,8 +371,14 @@
     ups = [(0, 1), (1, 2), (2, 3)]
     downs = [(3, 2), (2, 1), (1, 0)]
 
-    weights = [out_weight, along_tp(out_weight, 1), along_tp(out_weight, 2)]
-    weights.append(along_tp(weights[2], 1))
+    columns = out_weight.shape[1] // 2
+    cross = [along_tp(out_weight[:, :columns], 2), along_tp(out_weight[:, columns:], 2)]
+    weights = [
+        [out_weight],
+        [along_tp(out_weight, 1)],
+        cross,
+        [along_tp(cross[0], 1), along_tp(cross[1], 1)],
+    ]
     resid_up = along_outer(resid, ups)
     resid_down = along_outer(resid, downs)
 
@@ -386,7 +445,14 @@
             got.append(along_inner(sent, j))
         return got
 
+    second_up = along_outer(resid_up, ups[1:])
+    second_down = along_outer(resid_down, downs[1:])
+    near_resid = jnp.where(low, resid_down, resid_up)
+    spare_resid = jnp.where(
+        plane == 1, resid_up, jnp.where(plane == 2, resid_down, jnp.zeros_like(resid))
+    )
     other_resid = exchange(0, resid)
+    other_near_resid = exchange(1, near_resid)
 
     pooled = pool_mix(pool_in, pool_weight, pool_scale)
 
@@ -397,27 +463,44 @@
     pooled = jnp.concatenate(pieces, axis=1)
     pooled_up = along_outer(pooled, ups)
     pooled_down = along_outer(pooled, downs)
+    second_pooled = along_outer(pooled_up, ups[1:]) + along_outer(pooled_down, downs[1:])
+    near_pooled = jnp.where(low, pooled_down, pooled_up)
+    spare_pooled = jnp.where(
+        plane == 1, pooled_up, jnp.where(plane == 2, pooled_down, jnp.zeros_like(pooled))
+    )
     other_pooled = exchange(0, pooled)
-
-    up1, down1, near, spare = out_norm(
-        [pooled_up, pooled_down],
-        [resid_up, resid_down],
+    other_near_pooled = exchange(1, near_pooled)
+
+    normed, *other_normed, middle = out_norm(
+        [pooled, *other_pooled], [resid, *other_resid], norm_gain, weights, True
+    )
+    (second,) = out_norm(
+        [second_pooled], [second_up + second_down], norm_gain, weights, False
+    )
+    near, spare, *other_near = out_norm(
+        [near_pooled, spare_pooled, *other_near_pooled],
+        [near_resid, spare_resid, *other_near_resid],
         norm_gain,
         weights,
-        plane,
         False,
-        True,
-    )
-    normed, *other_normed, middle = out_norm(
-        [pooled, *other_pooled], [resid, *other_resid], norm_gain, weights, plane, True, False
-    )
-
-    up2 = along_outer(up1, ups[1:])
-    down2 = along_outer(down1, downs[1:])
-    up3 = along_outer(up2, ups[2:])
-    down3 = along_outer(down2, downs[2:])
-    lines = [normed, near, up2 + down2, spare + up3 + down3]
-    arrived = [other_normed] + [exchange(k, lines[k]) for k in (1, 2, 3)]
+    )
+
+    far = []
+    for h in range(2):
+        half = second[:, h * columns : (h + 1) * columns]
+        got_up = along_outer(half, ups[2:])
+        got_down = along_outer(half, downs[2:])
+        if far:
+            got_up, got_down, _ = lax.optimization_barrier((got_up, got_down, far[0]))
+        far.append(spare[:, h * columns : (h + 1) * columns] + got_up + got_down)
+
+    lines = [[normed], [near], [second], far]
+    arrived = [
+        [[o] for o in other_normed],
+        [[o] for o in other_near],
+        [[o] for o in exchange(2, second)],
+        [list(pair) for pair in zip(exchange(3, far[0]), exchange(3, far[1]))],
+    ]
     owns, backs = [], []
     for k in slots:
         own_table = group_of(k, 0)
@@ -435,8 +518,17 @@
         backs.append(back)
 
     def partial_sum(k):
-        parts = [along_inner(backs[k][j - 1], -j) for j in peers]
-        return combine(owns[k], send_mix[k], parts)
+        halves = []
+        whole = None
+        for h in range(2):
+            if len(backs[k][0]) == 2:
+                parts = [along_inner(backs[k][j - 1][h], -j) for j in peers]
+            else:
+                if whole is None:
+                    whole = [along_inner(backs[k][j - 1][0], -j) for j in peers]
+                parts = whole
+            halves.append(combine(owns[k], send_mix[k], parts, h))
+        return halves
 
     sums = [partial_sum(k) for k in slots]
 
@@ -444,21 +536,23 @@
         jax.nn.silu(jnp.dot(normed, shared_gate, preferred_element_type=f32))
         * jnp.dot(normed, shared_up, preferred_element_type=f32)
     ).astype(bf16)
-    base = middle.astype(f32) + jnp.dot(
-        shared_hidden, shared_down, preferred_element_type=f32
-    )
-
-    got_up = along_outer(sums[3], ups[:1])
-    got_down = along_outer(sums[3], downs[:1])
-    mid = sums[2] + got_up + got_down
-    got_up = along_outer(mid, ups[:2])
-    got_down = along_outer(mid, downs[:2])
-    near_up = jnp.where(plane == 2, sums[3], sums[1]) + got_up
-    near_down = jnp.where(plane == 1, sums[3], sums[1]) + got_down
-    got_up = along_outer(near_up, ups)
-    got_down = along_outer(near_down, downs)
-    base = base + sums[0].astype(f32)
-    return (base + got_up.astype(f32) + got_down.astype(f32)).astype(bf16)
+    base = lax.optimization_barrier(
+        middle.astype(f32)
+        + jnp.dot(shared_hidden, shared_down, preferred_element_type=f32)
+    )
+
+    last_up, last_down = [], []
+    for h in range(2):
+        got_up = along_outer(sums[3][h], ups[:1])
+        got_down = along_outer(sums[3][h], downs[:1])
+        mid = sums[2][h] + got_up + got_down
+        got_up = along_outer(mid, ups[:2])
+        got_down = along_outer(mid, downs[:2])
+        near_up = jnp.where(plane == 2, sums[3][h], sums[1][h]) + got_up
+        near_down = jnp.where(plane == 1, sums[3][h], sums[1][h]) + got_down
+        last_up.append(along_outer(near_up, ups))
+        last_down.append(along_outer(near_down, downs))
+    return finish(base, *sums[0], *last_up, *last_down)
 
 
 def solution(mesh):

time: 483 us -> 457 us (0.946)
  waiting for transfers between devices: 253 us -> 174 us
  starting transfers between devices: 62.9 us -> 102 us
  Pallas kernels: 105 us -> 123 us
    ppermute x9 -> x12, waiting for transfers between devices: 130 us -> 73.4 us  [along_inner(): return lax.ppermute(x, 'sp', pairs)]
    ppermute x17 -> x27, starting transfers between devices: 39.8 us -> 79.5 us  [along_outer(): return lax.ppermute(x, 'sp', pairs)]
    ppermute x17 -> x27, waiting for transfers between devices: 82.5 us -> 64.3 us  [along_outer(): return lax.ppermute(x, 'sp', pairs)]
    pallas_call x10 -> x16, Pallas kernels: 105 us -> 123 us  [the longest x4 85.6 us: run_experts(): pl.pallas_call(functools.partial(expert_kernel, peers, parts, capacity, p...]
    unnamed x90 -> x108, local copies, waits for them, and re-layouts: 13.6 us -> 6 us
    ppermute x6 -> x8, waiting for transfers between devices: 38.7 us -> 35.9 us  [along_tp(): return lax.ppermute(x, 'tp', [(i, i ^ bits) for i in range(n_tp)])]
    ppermute x9 -> x12, starting transfers between devices: 10.9 us -> 13 us  [along_inner(): return lax.ppermute(x, 'sp', pairs)]
    add x4 -> x8, other arithmetic: 11.5 us -> 10.4 us  [the longest x2 4.52 us: shards(): mid = sums[2][h] + got_up + got_down]
  transfers between devices with their start and end apart: 34 -> 49, of which waited for: 18 -> 13; matrix products, arithmetic and copies ran while one was open for 7% -> 11% of each run, Pallas kernels for 15% -> 26%
where the time goes in v1:
time: 457 us; the launch traced here: 456 us
  waiting for transfers between devices  174 us (38%)
  Pallas kernels  123 us (27%)
  starting transfers between devices  102 us (22%)
  matrix products  23.1 us (5%)
  other arithmetic  19.2 us (4%)
  local copies, waits for them, and re-layouts  14.4 us (3%)
    pallas_call x4, Pallas kernels, run_experts(): pl.pallas_call(functools.partial(expert_kernel, peers, parts, capacity, p...  85.6 us
    ppermute x27, starting transfers between devices, along_outer(): return lax.ppermute(x, 'sp', pairs)  79.5 us
    ppermute x12, waiting for transfers between devices, along_inner(): return lax.ppermute(x, 'sp', pairs)  73.4 us
    ppermute x27, waiting for transfers between devices, along_outer(): return lax.ppermute(x, 'sp', pairs)  64.3 us
    ppermute x8, waiting for transfers between devices, along_tp(): return lax.ppermute(x, 'tp', [(i, i ^ bits) for i in range(n_tp)])  35.9 us
    pallas_call x3, Pallas kernels, out_norm(): pl.pallas_call(functools.partial(out_norm_kernel, blocks, keep, [len(g) f...  23.1 us
    ppermute x12, starting transfers between devices, along_inner(): return lax.ppermute(x, 'sp', pairs)  13 us
    pallas_call x8, Pallas kernels, combine(): pl.pallas_call(functools.partial(combine_kernel, count), grid=(2,), out_s...  10.3 us
  transfers between devices with their start and end apart: 49, of which 13 were waited for; matrix products, arithmetic and copies ran while one was open for 11% of the time, Pallas kernels for 26%

profile of v1, /device:TPU:0, one launch (start us, length us, event | category | flops | bytes accessed | tf_op | source)
XLA Modules:
  0.0 455.8 jit_solution(14637871224711046876)
XLA Ops:
  0.0 6.4 %collective-permute-start.19 = (bf16[192,4096]{1,0:T(8,128)(2,1)}, bf16[192,4096]{1,0:T(8,128)(2,1)}, u32[]{:S(2)}, u32[]{:S(2)}) collective-permute-start(bf16[192,4096]{1,0:T(8,128)(2,1)} %refs_2_.1), channel_id=1, source_target_pairs={{0,8},{4,12},{8,16},{12,20},{16,24},{20,28},{1,9},{5,13},{9,17},{1... | collective-permute-start | bytes 4718600 | tf_op jit(solution)/shard_map/ppermute | solution.py:358
  9.0 4.0 collective-permute-start
  18.4 3.3 fusion.46
  30.2 3.2 collective-permute-done.4
  33.4 19.3 %collective-permute-start.33 = (f32[2,8,192]{2,1,0:T(8,128)S(1)}, f32[2,8,192]{2,1,0:T(8,128)S(1)}, u32[]{:S(2)}, u32[]{:S(2)}) collective-permute-start(f32[2,8,192]{2,1,0:T(8,128)S(1)} %copy-done.45), channel_id=1, source_target_pairs={{0,16},{4,20},{8,24},{12,28},{16,0},{20,4},{24,8},{28,12},{1,17},{... | collective-permute-start | bytes 36872 | tf_op jit(solution)/shard_map/ppermute | solution.py:358
  52.7 3.2 collective-permute-start.15
  58.1 5.3 %collective-permute-start.14 = (bf16[192,1024]{1,0:T(8,128)(2,1)S(1)}, bf16[192,1024]{1,0:T(8,128)(2,1)}, u32[]{:S(2)}, u32[]{:S(2)}) collective-permute-start(bf16[192,1024]{1,0:T(8,128)(2,1)S(1)} %pad_maximum_fusion.refs_0_), channel_id=1, source_target_pairs={{0,8},{4,12},{8,16},{12,20},{16,24},{20,28},{1,9},{5,13},{9,17},{1... | collective-permute-start | bytes 1179656 | tf_op jit(solution)/shard_map/ppermute | solution.py:358
  64.9 3.9 collective-permute-done.13
  74.6 6.4 %collective-permute-done.22 = bf16[192,1024]{1,0:T(8,128)(2,1)} collective-permute-done((bf16[192,1024]{1,0:T(8,128)(2,1)}, bf16[192,1024]{1,0:T(8,128)(2,1)}, u32[]{:S(2)}, u32[]{:S(2)}) %collective-permute-start.22) | collective-permute-done | bytes 393248 | tf_op jit(solution)/shard_map/ppermute | solution.py:358
  85.0 12.4 %collective-permute-done.9.refs_8_.refs_10_.refs_6_ = bf16[256,2048]{1,0:T(8,128)(2,1)} collective-permute-done((bf16[256,2048]{1,0:T(8,128)(2,1)}, bf16[256,2048]{1,0:T(8,128)(2,1)}, u32[]{:S(2)}, u32[]{:S(2)}) %collective-permute-start.9) | collective-permute-done | bytes 1048608 | tf_op jit(solution)/shard_map/ppermute | solution.py:369
  97.4 20.3 %collective-permute-done.8.refs_7_.refs_9_.refs_5_ = bf16[256,2048]{1,0:T(8,128)(2,1)} collective-permute-done((bf16[256,2048]{1,0:T(8,128)(2,1)}, bf16[256,2048]{1,0:T(8,128)(2,1)}, u32[]{:S(2)}, u32[]{:S(2)}) %collective-permute-start.8) | collective-permute-done | bytes 1048608 | tf_op jit(solution)/shard_map/ppermute | solution.py:369
  125.5 31.8 %collective-permute-done.24 = bf16[192,4096]{1,0:T(8,128)(2,1)S(1)} collective-permute-done((bf16[192,4096]{1,0:T(8,128)(2,1)}, bf16[192,4096]{1,0:T(8,128)(2,1)S(1)}, u32[]{:S(2)}, u32[]{:S(2)}) %collective-permute-start.24) | collective-permute-done | bytes 1572896 | tf_op jit(solution)/shard_map/ppermute | solution.py:358
  160.0 5.1 %out_norm.5.refs_0_ = bf16[192,4096]{1,0:T(8,128)(2,1)S(1)} custom-call(bf16[192,1024]{1,0:T(8,128)(2,1)S(1)} %add.322.refs_0_, bf16[192,4096]{1,0:T(8,128)(2,1)S(1)} %add.323.refs_1_, f32[1,4096]{1,0:T(1,128)S(1)} %bitcast.86, bf16[256,4096]{1,0:T(8,128)(2,1)S(1)} %copy-done.1, bf16[256,4096]{1,0:T(8,128)(2,1)S(1)} %collective-permute-done.7.refs_6_.refs_8_.refs_4_, ...), custom_call_target="tpu_custom_call" | custom-call | flops 1610612736 | bytes 3145728 | tf_op jit(solution)/shard_map/out_norm/pallas_call | solution.py:125
  167.5 24.1 %collective-permute-done.17.refs_2_ = bf16[144,1024]{1,0:T(8,128)(2,1)S(1)} collective-permute-done((bf16[144,1024]{1,0:T(8,128)(2,1)S(1)}, bf16[144,1024]{1,0:T(8,128)(2,1)S(1)}, u32[]{:S(2)}, u32[]{:S(2)}) %collective-permute-start.17) | collective-permute-done | bytes 294944 | tf_op jit(solution)/shard_map/ppermute | solution.py:366
  191.7 10.5 %out_norm.4 = (bf16[192,4096]{1,0:T(8,128)(2,1)S(1)}, bf16[192,4096]{1,0:T(8,128)(2,1)S(1)}, bf16[144,4096]{1,0:T(8,128)(2,1)S(1)}) custom-call(bf16[192,1024]{1,0:T(8,128)(2,1)S(1)} %get-tuple-element.50.refs_0_, bf16[192,1024]{1,0:T(8,128)(2,1)S(1)} %get-tuple-element.49.refs_1_, bf16[144,1024]{1,0:T(8,128)(2,1)S(1)} %collective-permute-done.17.refs_2_, ...), custom_call_target="tpu_custom_call" | custom-call | flops 4429185024 | bytes 8650752 | tf_op jit(solution)/shard_map/out_norm/pallas_call | solution.py:125
  207.4 15.2 %collective-permute-done.28 = bf16[192,2048]{1,0:T(8,128)(2,1)S(1)} collective-permute-done((bf16[192,2048]{1,0:T(8,128)(2,1)S(1)}, bf16[192,2048]{1,0:T(8,128)(2,1)S(1)}, u32[]{:S(2)}, u32[]{:S(2)}) %collective-permute-start.28) | collective-permute-done | bytes 786464 | tf_op jit(solution)/shard_map/ppermute | solution.py:358
  226.4 21.2 %collective-permute-done.29.refs_2_ = bf16[144,2048]{1,0:T(8,128)(2,1)S(1)} collective-permute-done((bf16[144,2048]{1,0:T(8,128)(2,1)S(1)}, bf16[144,2048]{1,0:T(8,128)(2,1)S(1)}, u32[]{:S(2)}, u32[]{:S(2)}) %collective-permute-start.29) | collective-permute-done | bytes 589856 | tf_op jit(solution)/shard_map/ppermute | solution.py:366
  247.6 10.7 %collective-permute-done.30.refs_3_ = bf16[144,2048]{1,0:T(8,128)(2,1)S(1)} collective-permute-done((bf16[144,2048]{1,0:T(8,128)(2,1)S(1)}, bf16[144,2048]{1,0:T(8,128)(2,1)S(1)}, u32[]{:S(2)}, u32[]{:S(2)}) %collective-permute-start.30) | collective-permute-done | bytes 589856 | tf_op jit(solution)/shard_map/ppermute | solution.py:366
  258.4 21.3 %experts.5 = (f32[192,4096]{1,0:T(8,128)}, bf16[144,2048]{1,0:T(8,128)(2,1)S(1)}, bf16[144,2048]{1,0:T(8,128)(2,1)}) custom-call(bf16[192,2048]{1,0:T(8,128)(2,1)S(1)} %add_add_fusion.3.refs_0_, bf16[192,2048]{1,0:T(8,128)(2,1)S(1)} %add_add_fusion.2.refs_1_, bf16[144,2048]{1,0:T(8,128)(2,1)S(1)} %collective-permute-done.29.refs_2_, ...), custom_call_target="tpu_custom_call" | custom-call | flops 3623878656 | bytes 37748736 | tf_op jit(solution)/shard_map/experts/pallas_call | solution.py:304
  285.8 21.6 %experts.7 = (f32[192,4096]{1,0:T(8,128)}, bf16[144,4096]{1,0:T(8,128)(2,1)}) custom-call(bf16[192,4096]{1,0:T(8,128)(2,1)S(1)} %out_norm.5.refs_0_, bf16[144,4096]{1,0:T(8,128)(2,1)S(1)} %copy-done.22, f32[4,192]{1,0:T(4,128)S(1)} %get-tuple-element.65.refs_2_, f32[4,192]{1,0:T(4,128)S(1)} %get-tuple-element.64.refs_3_, bf16[4,4096,384]{2,1,0:T(8,128)(2,1)} %refs_4_.5, ...), custom_call_target="tpu_custom_call" | custom-call | flops 3623878656 | bytes 37748736 | tf_op jit(solution)/shard_map/experts/pallas_call | solution.py:304
  313.8 5.2 %collective-permute-start.41 = (bf16[192,2048]{1,0:T(8,128)(2,1)}, bf16[192,2048]{1,0:T(8,128)(2,1)}, u32[]{:S(2)}, u32[]{:S(2)}) collective-permute-start(bf16[192,2048]{1,0:T(8,128)(2,1)} %combine.13), channel_id=1, source_target_pairs={{0,8},{4,12},{1,9},{5,13},{2,10},{6,14},{3,11},{7,15}} | collective-permute-start | bytes 2359304 | tf_op jit(solution)/shard_map/ppermute | solution.py:358
  319.9 7.5 %out_norm.3 = (bf16[192,4096]{1,0:T(8,128)(2,1)S(1)}, bf16[144,4096]{1,0:T(8,128)(2,1)S(1)}, bf16[192,4096]{1,0:T(8,128)(2,1)S(1)}) custom-call(bf16[192,1024]{1,0:T(8,128)(2,1)S(1)} %copy-done.15, bf16[144,1024]{1,0:T(8,128)(2,1)} %collective-permute-done.5.refs_1_, bf16[192,4096]{1,0:T(8,128)(2,1)S(1)} %copy-done.9, ...), custom_call_target="tpu_custom_call" | custom-call | flops 2818572288 | bytes 5505024 | tf_op jit(solution)/shard_map/out_norm/pallas_call | solution.py:125
  328.5 17.3 %collective-permute-done.31.refs_1_ = bf16[144,2048]{1,0:T(8,128)(2,1)S(1)} collective-permute-done((bf16[144,2048]{1,0:T(8,128)(2,1)}, bf16[144,2048]{1,0:T(8,128)(2,1)S(1)}, u32[]{:S(2)}, u32[]{:S(2)}) %collective-permute-start.31) | collective-permute-done | bytes 589856 | tf_op jit(solution)/shard_map/ppermute | solution.py:366
  348.2 4.9 %collective-permute-start.36 = (bf16[192,2048]{1,0:T(8,128)(2,1)S(1)}, bf16[192,2048]{1,0:T(8,128)(2,1)}, u32[]{:S(2)}, u32[]{:S(2)}) collective-permute-start(bf16[192,2048]{1,0:T(8,128)(2,1)S(1)} %combine.10), channel_id=1, source_target_pairs={{0,8},{4,12},{1,9},{5,13},{2,10},{6,14},{3,11},{7,15}} | collective-permute-start | bytes 2359304 | tf_op jit(solution)/shard_map/ppermute | solution.py:358
  353.1 21.1 %experts.6 = (f32[192,4096]{1,0:T(8,128)}, bf16[144,4096]{1,0:T(8,128)(2,1)S(1)}) custom-call(bf16[192,4096]{1,0:T(8,128)(2,1)S(1)} %copy-done.13, bf16[144,4096]{1,0:T(8,128)(2,1)S(1)} %copy-done.18, f32[4,192]{1,0:T(4,128)S(1)} %get-tuple-element.63.refs_2_, f32[4,192]{1,0:T(4,128)S(1)} %get-tuple-element.62.refs_3_, bf16[4,4096,384]{2,1,0:T(8,128)(2,1)} %refs_4_.5, ...), custom_call_target="tpu_custom_call" | custom-call | flops 3623878656 | bytes 37748736 | tf_op jit(solution)/shard_map/experts/pallas_call | solution.py:304
  384.8 5.1 %collective-permute-start.38 = (bf16[192,2048]{1,0:T(8,128)(2,1)}, bf16[192,2048]{1,0:T(8,128)(2,1)S(1)}, u32[]{:S(2)}, u32[]{:S(2)}) collective-permute-start(bf16[192,2048]{1,0:T(8,128)(2,1)} %add_add_fusion.1), channel_id=1, source_target_pairs={{0,8},{4,12},{8,16},{12,20},{1,9},{5,13},{9,17},{13,21},{2,10},{6,... | collective-permute-start | bytes 2359304 | tf_op jit(solution)/shard_map/ppermute | solution.py:358
  389.9 21.6 %experts.4 = (f32[192,4096]{1,0:T(8,128)}, bf16[144,4096]{1,0:T(8,128)(2,1)}) custom-call(bf16[192,4096]{1,0:T(8,128)(2,1)S(1)} %get-tuple-element.23.refs_0_, bf16[144,4096]{1,0:T(8,128)(2,1)S(1)} %copy-done.20, f32[4,192]{1,0:T(4,128)S(1)} %get-tuple-element.69.refs_2_, f32[4,192]{1,0:T(4,128)S(1)} %get-tuple-element.68.refs_3_, ...), custom_call_target="tpu_custom_call" | custom-call | flops 3623878656 | bytes 37748736 | tf_op jit(solution)/shard_map/experts/pallas_call | solution.py:304
  417.8 6.3 %collective-permute-start.44 = (bf16[192,2048]{1,0:T(8,128)(2,1)}, bf16[192,2048]{1,0:T(8,128)(2,1)}, u32[]{:S(2)}, u32[]{:S(2)}) collective-permute-start(bf16[192,2048]{1,0:T(8,128)(2,1)} %get-tuple-element.44), channel_id=1, source_target_pairs={{0,8},{4,12},{8,16},{12,20},{16,24},{20,28},{1,9},{5,13},{9,17},{1... | collective-permute-start | bytes 2359304 | tf_op jit(solution)/shard_map/ppermute | solution.py:358
  426.8 5.5 %collective-permute-start.39 = (bf16[192,2048]{1,0:T(8,128)(2,1)}, bf16[192,2048]{1,0:T(8,128)(2,1)}, u32[]{:S(2)}, u32[]{:S(2)}) collective-permute-start(bf16[192,2048]{1,0:T(8,128)(2,1)} %get-tuple-element.46), channel_id=1, source_target_pairs={{0,8},{4,12},{8,16},{12,20},{16,24},{20,28},{1,9},{5,13},{9,17},{1... | collective-permute-start | bytes 2359304 | tf_op jit(solution)/shard_map/ppermute | solution.py:358
  433.3 6.4 %convert_add_fusion.base = f32[192,4096]{1,0:T(8,128)} fusion(bf16[192,4096]{1,0:T(8,128)(2,1)} %copy-done.16, bf16[384,4096]{1,0:T(8,128)(2,1)S(1)} %copy-done, f32[192,384]{1,0:T(8,128)S(1)} %fusion.53, bf16[192,4096]{1,0:T(8,128)(2,1)} %copy-done.2, bf16[4096,384]{1,0:T(8,128)(2,1)} %param.26), kind=kOutput, calls=%fused_computation.3 | convolution fusion | flops 1209974784 | bytes 12877824 | tf_op jit(solution)/shard_map/dot_general | solution.py:541
  445.3 5.5 %collective-permute-done.46.down_a = bf16[192,2048]{1,0:T(8,128)(2,1)} collective-permute-done((bf16[192,2048]{1,0:T(8,128)(2,1)}, bf16[192,2048]{1,0:T(8,128)(2,1)}, u32[]{:S(2)}, u32[]{:S(2)}) %collective-permute-start.46) | collective-permute-done | bytes 786464 | tf_op jit(solution)/shard_map/ppermute | solution.py:358
  452.2 3.6 finish.1
  (243 shorter events, 95.7 us)
Async XLA Ops:
  0.0 83.3 %collective-permute-start.19 = (bf16[192,4096]{1,0:T(8,128)(2,1)}, bf16[192,4096]{1,0:T(8,128)(2,1)}, u32[]{:S(2)}, u32[]{:S(2)}) collective-permute-start(bf16[192,4096]{1,0:T(8,128)(2,1)} %refs_2_.1), channel_id=1, source_target_pairs={{0,8},{4,12},{8,16},{12,20},{16,24},{20,28},{1,9},{5,13},{9,17},{1... | collective-permute-start | bytes 4718600 | tf_op jit(solution)/shard_map/ppermute | solution.py:358
  6.4 111.3 %collective-permute-start.18 = (bf16[192,4096]{1,0:T(8,128)(2,1)}, bf16[192,4096]{1,0:T(8,128)(2,1)}, u32[]{:S(2)}, u32[]{:S(2)}) collective-permute-start(bf16[192,4096]{1,0:T(8,128)(2,1)} %refs_2_.1), channel_id=1, source_target_pairs={{24,16},{28,20},{16,8},{20,12},{8,0},{12,4},{25,17},{29,21},{17,9}... | collective-permute-start | bytes 4718600 | tf_op jit(solution)/shard_map/ppermute | solution.py:358
  71.1 26.3 %collective-permute-start.9 = (bf16[256,2048]{1,0:T(8,128)(2,1)}, bf16[256,2048]{1,0:T(8,128)(2,1)}, u32[]{:S(2)}, u32[]{:S(2)}) collective-permute-start(bf16[256,2048]{1,0:T(8,128)(2,1)} %get-tuple-element.41), channel_id=1, source_target_pairs={{0,2},{1,3},{2,0},{3,1},{4,6},{5,7},{6,4},{7,5},{8,10},{9,11},{10,... | collective-permute-start | bytes 3145736 | tf_op jit(solution)/shard_map/ppermute | solution.py:369
  71.4 46.3 %collective-permute-start.8 = (bf16[256,2048]{1,0:T(8,128)(2,1)}, bf16[256,2048]{1,0:T(8,128)(2,1)}, u32[]{:S(2)}, u32[]{:S(2)}) collective-permute-start(bf16[256,2048]{1,0:T(8,128)(2,1)} %get-tuple-element.42), channel_id=1, source_target_pairs={{0,2},{1,3},{2,0},{3,1},{4,6},{5,7},{6,4},{7,5},{8,10},{9,11},{10,... | collective-permute-start | bytes 3145736 | tf_op jit(solution)/shard_map/ppermute | solution.py:369
  82.5 77.4 %collective-permute-start.7 = (bf16[256,4096]{1,0:T(8,128)(2,1)}, bf16[256,4096]{1,0:T(8,128)(2,1)S(1)}, u32[]{:S(2)}, u32[]{:S(2)}) collective-permute-start(bf16[256,4096]{1,0:T(8,128)(2,1)} %refs_3_.1), channel_id=1, source_target_pairs={{0,1},{1,0},{2,3},{3,2},{4,5},{5,4},{6,7},{7,6},{8,9},{9,8},{10,11... | collective-permute-start | bytes 6291464 | tf_op jit(solution)/shard_map/ppermute | solution.py:369
  83.3 38.2 %collective-permute-start.23 = (bf16[192,4096]{1,0:T(8,128)(2,1)}, bf16[192,4096]{1,0:T(8,128)(2,1)S(1)}, u32[]{:S(2)}, u32[]{:S(2)}) collective-permute-start(bf16[192,4096]{1,0:T(8,128)(2,1)} %collective-permute-done.19), channel_id=1, source_target_pairs={{8,16},{12,20},{16,24},{20,28},{9,17},{13,21},{17,25},{21,29},{10,... | collective-permute-start | bytes 4718600 | tf_op jit(solution)/shard_map/ppermute | solution.py:358
  97.4 61.8 %collective-permute-start.11 = (bf16[256,2048]{1,0:T(8,128)(2,1)}, bf16[256,2048]{1,0:T(8,128)(2,1)S(1)}, u32[]{:S(2)}, u32[]{:S(2)}) collective-permute-start(bf16[256,2048]{1,0:T(8,128)(2,1)} %collective-permute-done.9.refs_8_.refs_10_.refs_6_), channel_id=1, source_target_pairs={{0,1},{1,0},{2,3},{3,2},{4,5},{5,4},{6,7},{7,6},{8,9},{9,8},{10,11... | collective-permute-start | bytes 3145736 | tf_op jit(solution)/shard_map/ppermute | solution.py:369
  117.7 42.3 %collective-permute-start.10 = (bf16[256,2048]{1,0:T(8,128)(2,1)}, bf16[256,2048]{1,0:T(8,128)(2,1)S(1)}, u32[]{:S(2)}, u32[]{:S(2)}) collective-permute-start(bf16[256,2048]{1,0:T(8,128)(2,1)} %collective-permute-done.8.refs_7_.refs_9_.refs_5_), channel_id=1, source_target_pairs={{0,1},{1,0},{2,3},{3,2},{4,5},{5,4},{6,7},{7,6},{8,9},{9,8},{10,11... | collective-permute-start | bytes 3145736 | tf_op jit(solution)/shard_map/ppermute | solution.py:369
  117.7 39.6 %collective-permute-start.24 = (bf16[192,4096]{1,0:T(8,128)(2,1)}, bf16[192,4096]{1,0:T(8,128)(2,1)S(1)}, u32[]{:S(2)}, u32[]{:S(2)}) collective-permute-start(bf16[192,4096]{1,0:T(8,128)(2,1)} %collective-permute-done.18), channel_id=1, source_target_pairs={{16,8},{20,12},{8,0},{12,4},{17,9},{21,13},{9,1},{13,5},{18,10},{2... | collective-permute-start | bytes 4718600 | tf_op jit(solution)/shard_map/ppermute | solution.py:358
  121.6 70.1 %collective-permute-start.20 = (bf16[144,4096]{1,0:T(8,128)(2,1)S(1)}, bf16[144,4096]{1,0:T(8,128)(2,1)S(1)}, u32[]{:S(2)}, u32[]{:S(2)}) collective-permute-start(bf16[144,4096]{1,0:T(8,128)(2,1)S(1)} %convolution_convert_fusion.1), channel_id=1, source_target_pairs={{0,4},{4,0},{8,12},{12,8},{16,20},{20,16},{24,28},{28,24},{1,5},{5... | collective-permute-start | bytes 3538952 | tf_op jit(solution)/shard_map/ppermute | solution.py:366
  157.3 162.6 %collective-permute-start.6 = (bf16[144,4096]{1,0:T(8,128)(2,1)}, bf16[144,4096]{1,0:T(8,128)(2,1)S(1)}, u32[]{:S(2)}, u32[]{:S(2)}) collective-permute-start(bf16[144,4096]{1,0:T(8,128)(2,1)} %convolution_convert_fusion.2), channel_id=1, source_target_pairs={{0,4},{4,0},{8,12},{12,8},{16,20},{20,16},{24,28},{28,24},{1,5},{5... | collective-permute-start | bytes 3538952 | tf_op jit(solution)/shard_map/ppermute | solution.py:366
  159.2 32.5 %collective-permute-start.17 = (bf16[144,1024]{1,0:T(8,128)(2,1)S(1)}, bf16[144,1024]{1,0:T(8,128)(2,1)S(1)}, u32[]{:S(2)}, u32[]{:S(2)}) collective-permute-start(bf16[144,1024]{1,0:T(8,128)(2,1)S(1)} %convolution_convert_fusion.5), channel_id=1, source_target_pairs={{0,4},{4,0},{8,12},{12,8},{16,20},{20,16},{24,28},{28,24},{1,5},{5... | collective-permute-start | bytes 884744 | tf_op jit(solution)/shard_map/ppermute | solution.py:366
  165.3 40.6 %collective-permute-start.26 = (bf16[192,2048]{1,0:T(8,128)(2,1)S(1)}, bf16[192,2048]{1,0:T(8,128)(2,1)S(1)}, u32[]{:S(2)}, u32[]{:S(2)}) collective-permute-start(bf16[192,2048]{1,0:T(8,128)(2,1)S(1)} %get-tuple-element.48), channel_id=1, source_target_pairs={{8,0},{12,4},{9,1},{13,5},{10,2},{14,6},{11,3},{15,7}} | collective-permute-start | bytes 2359304 | tf_op jit(solution)/shard_map/ppermute | solution.py:358
  166.6 40.7 %collective-permute-start.25 = (bf16[192,2048]{1,0:T(8,128)(2,1)S(1)}, bf16[192,2048]{1,0:T(8,128)(2,1)S(1)}, u32[]{:S(2)}, u32[]{:S(2)}) collective-permute-start(bf16[192,2048]{1,0:T(8,128)(2,1)S(1)} %get-tuple-element.48), channel_id=1, source_target_pairs={{16,24},{20,28},{17,25},{21,29},{18,26},{22,30},{19,27},{23,31}} | collective-permute-start | bytes 2359304 | tf_op jit(solution)/shard_map/ppermute | solution.py:358
  205.9 77.6 %collective-permute-start.34 = (bf16[144,4096]{1,0:T(8,128)(2,1)}, bf16[144,4096]{1,0:T(8,128)(2,1)S(1)}, u32[]{:S(2)}, u32[]{:S(2)}) collective-permute-start(bf16[144,4096]{1,0:T(8,128)(2,1)} %convolution_convert_fusion), channel_id=1, source_target_pairs={{0,4},{4,0},{8,12},{12,8},{16,20},{20,16},{24,28},{28,24},{1,5},{5... | collective-permute-start | bytes 3538952 | tf_op jit(solution)/shard_map/ppermute | solution.py:366
  224.8 33.5 %collective-permute-start.30 = (bf16[144,2048]{1,0:T(8,128)(2,1)S(1)}, bf16[144,2048]{1,0:T(8,128)(2,1)S(1)}, u32[]{:S(2)}, u32[]{:S(2)}) collective-permute-start(bf16[144,2048]{1,0:T(8,128)(2,1)S(1)} %convolution_convert_fusion.3), channel_id=1, source_target_pairs={{0,4},{4,0},{8,12},{12,8},{16,20},{20,16},{24,28},{28,24},{1,5},{5... | collective-permute-start | bytes 1769480 | tf_op jit(solution)/shard_map/ppermute | solution.py:366
  279.6 30.9 %collective-permute-start.40 = (bf16[144,2048]{1,0:T(8,128)(2,1)}, bf16[144,2048]{1,0:T(8,128)(2,1)}, u32[]{:S(2)}, u32[]{:S(2)}) collective-permute-start(bf16[144,2048]{1,0:T(8,128)(2,1)} %get-tuple-element.38), channel_id=1, source_target_pairs={{0,4},{4,0},{8,12},{12,8},{16,20},{20,16},{24,28},{28,24},{1,5},{5... | collective-permute-start | bytes 1769480 | tf_op jit(solution)/shard_map/ppermute | solution.py:366
  282.8 31.0 %collective-permute-start.5 = (bf16[144,1024]{1,0:T(8,128)(2,1)}, bf16[144,1024]{1,0:T(8,128)(2,1)}, u32[]{:S(2)}, u32[]{:S(2)}) collective-permute-start(bf16[144,1024]{1,0:T(8,128)(2,1)} %convolution_convert_fusion.6), channel_id=1, source_target_pairs={{0,4},{4,0},{8,12},{12,8},{16,20},{20,16},{24,28},{28,24},{1,5},{5... | collective-permute-start | bytes 884744 | tf_op jit(solution)/shard_map/ppermute | solution.py:366
  307.4 66.9 %collective-permute-start.35 = (bf16[144,4096]{1,0:T(8,128)(2,1)}, bf16[144,4096]{1,0:T(8,128)(2,1)S(1)}, u32[]{:S(2)}, u32[]{:S(2)}) collective-permute-start(bf16[144,4096]{1,0:T(8,128)(2,1)} %get-tuple-element.37), channel_id=1, source_target_pairs={{0,4},{4,0},{8,12},{12,8},{16,20},{20,16},{24,28},{28,24},{1,5},{5... | collective-permute-start | bytes 3538952 | tf_op jit(solution)/shard_map/ppermute | solution.py:366
  309.7 36.1 %collective-permute-start.31 = (bf16[144,2048]{1,0:T(8,128)(2,1)}, bf16[144,2048]{1,0:T(8,128)(2,1)S(1)}, u32[]{:S(2)}, u32[]{:S(2)}) collective-permute-start(bf16[144,2048]{1,0:T(8,128)(2,1)} %copy-done.27), channel_id=1, source_target_pairs={{0,4},{4,0},{8,12},{12,8},{16,20},{20,16},{24,28},{28,24},{1,5},{5... | collective-permute-start | bytes 1769480 | tf_op jit(solution)/shard_map/ppermute | solution.py:366
  313.1 64.2 %collective-permute-start.42 = (bf16[192,2048]{1,0:T(8,128)(2,1)}, bf16[192,2048]{1,0:T(8,128)(2,1)S(1)}, u32[]{:S(2)}, u32[]{:S(2)}) collective-permute-start(bf16[192,2048]{1,0:T(8,128)(2,1)} %combine.13), channel_id=1, source_target_pairs={{24,16},{28,20},{25,17},{29,21},{26,18},{30,22},{27,19},{31,23}} | collective-permute-start | bytes 2359304 | tf_op jit(solution)/shard_map/ppermute | solution.py:358
  313.8 63.5 %collective-permute-start.41 = (bf16[192,2048]{1,0:T(8,128)(2,1)}, bf16[192,2048]{1,0:T(8,128)(2,1)}, u32[]{:S(2)}, u32[]{:S(2)}) collective-permute-start(bf16[192,2048]{1,0:T(8,128)(2,1)} %combine.13), channel_id=1, source_target_pairs={{0,8},{4,12},{1,9},{5,13},{2,10},{6,14},{3,11},{7,15}} | collective-permute-start | bytes 2359304 | tf_op jit(solution)/shard_map/ppermute | solution.py:358
  346.7 35.0 %collective-permute-start.37 = (bf16[192,2048]{1,0:T(8,128)(2,1)S(1)}, bf16[192,2048]{1,0:T(8,128)(2,1)}, u32[]{:S(2)}, u32[]{:S(2)}) collective-permute-start(bf16[192,2048]{1,0:T(8,128)(2,1)S(1)} %combine.10), channel_id=1, source_target_pairs={{24,16},{28,20},{25,17},{29,21},{26,18},{30,22},{27,19},{31,23}} | collective-permute-start | bytes 2359304 | tf_op jit(solution)/shard_map/ppermute | solution.py:358
  348.2 33.4 %collective-permute-start.36 = (bf16[192,2048]{1,0:T(8,128)(2,1)S(1)}, bf16[192,2048]{1,0:T(8,128)(2,1)}, u32[]{:S(2)}, u32[]{:S(2)}) collective-permute-start(bf16[192,2048]{1,0:T(8,128)(2,1)S(1)} %combine.10), channel_id=1, source_target_pairs={{0,8},{4,12},{1,9},{5,13},{2,10},{6,14},{3,11},{7,15}} | collective-permute-start | bytes 2359304 | tf_op jit(solution)/shard_map/ppermute | solution.py:358
  374.3 37.2 %collective-permute-start.32 = (bf16[144,4096]{1,0:T(8,128)(2,1)S(1)}, bf16[144,4096]{1,0:T(8,128)(2,1)S(1)}, u32[]{:S(2)}, u32[]{:S(2)}) collective-permute-start(bf16[144,4096]{1,0:T(8,128)(2,1)S(1)} %get-tuple-element.35), channel_id=1, source_target_pairs={{0,4},{4,0},{8,12},{12,8},{16,20},{20,16},{24,28},{28,24},{1,5},{5... | collective-permute-start | bytes 3538952 | tf_op jit(solution)/shard_map/ppermute | solution.py:366
  379.5 34.5 %collective-permute-start.47 = (bf16[192,2048]{1,0:T(8,128)(2,1)}, bf16[192,2048]{1,0:T(8,128)(2,1)S(1)}, u32[]{:S(2)}, u32[]{:S(2)}) collective-permute-start(bf16[192,2048]{1,0:T(8,128)(2,1)} %add_add_fusion), channel_id=1, source_target_pairs={{24,16},{28,20},{16,8},{20,12},{25,17},{29,21},{17,9},{21,13},{26,... | collective-permute-start | bytes 2359304 | tf_op jit(solution)/shard_map/ppermute | solution.py:358
  380.3 33.6 %collective-permute-start.43 = (bf16[192,2048]{1,0:T(8,128)(2,1)}, bf16[192,2048]{1,0:T(8,128)(2,1)S(1)}, u32[]{:S(2)}, u32[]{:S(2)}) collective-permute-start(bf16[192,2048]{1,0:T(8,128)(2,1)} %add_add_fusion), channel_id=1, source_target_pairs={{0,8},{4,12},{8,16},{12,20},{1,9},{5,13},{9,17},{13,21},{2,10},{6,... | collective-permute-start | bytes 2359304 | tf_op jit(solution)/shard_map/ppermute | solution.py:358
  384.1 40.1 %collective-permute-start.45 = (bf16[192,2048]{1,0:T(8,128)(2,1)}, bf16[192,2048]{1,0:T(8,128)(2,1)S(1)}, u32[]{:S(2)}, u32[]{:S(2)}) collective-permute-start(bf16[192,2048]{1,0:T(8,128)(2,1)} %add_add_fusion.1), channel_id=1, source_target_pairs={{24,16},{28,20},{16,8},{20,12},{25,17},{29,21},{17,9},{21,13},{26,... | collective-permute-start | bytes 2359304 | tf_op jit(solution)/shard_map/ppermute | solution.py:358
  384.8 39.4 %collective-permute-start.38 = (bf16[192,2048]{1,0:T(8,128)(2,1)}, bf16[192,2048]{1,0:T(8,128)(2,1)S(1)}, u32[]{:S(2)}, u32[]{:S(2)}) collective-permute-start(bf16[192,2048]{1,0:T(8,128)(2,1)} %add_add_fusion.1), channel_id=1, source_target_pairs={{0,8},{4,12},{8,16},{12,20},{1,9},{5,13},{9,17},{13,21},{2,10},{6,... | collective-permute-start | bytes 2359304 | tf_op jit(solution)/shard_map/ppermute | solution.py:358
  411.5 28.3 %collective-permute-start.12 = (bf16[144,4096]{1,0:T(8,128)(2,1)}, bf16[144,4096]{1,0:T(8,128)(2,1)}, u32[]{:S(2)}, u32[]{:S(2)}) collective-permute-start(bf16[144,4096]{1,0:T(8,128)(2,1)} %get-tuple-element.26), channel_id=1, source_target_pairs={{0,4},{4,0},{8,12},{12,8},{16,20},{20,16},{24,28},{28,24},{1,5},{5... | collective-permute-start | bytes 3538952 | tf_op jit(solution)/shard_map/ppermute | solution.py:366
  416.5 28.7 %collective-permute-start.48 = (bf16[192,2048]{1,0:T(8,128)(2,1)}, bf16[192,2048]{1,0:T(8,128)(2,1)}, u32[]{:S(2)}, u32[]{:S(2)}) collective-permute-start(bf16[192,2048]{1,0:T(8,128)(2,1)} %get-tuple-element.43), channel_id=1, source_target_pairs={{24,16},{28,20},{16,8},{20,12},{8,0},{12,4},{25,17},{29,21},{17,9}... | collective-permute-start | bytes 2359304 | tf_op jit(solution)/shard_map/ppermute | solution.py:358
  417.8 27.4 %collective-permute-start.44 = (bf16[192,2048]{1,0:T(8,128)(2,1)}, bf16[192,2048]{1,0:T(8,128)(2,1)}, u32[]{:S(2)}, u32[]{:S(2)}) collective-permute-start(bf16[192,2048]{1,0:T(8,128)(2,1)} %get-tuple-element.44), channel_id=1, source_target_pairs={{0,8},{4,12},{8,16},{12,20},{16,24},{20,28},{1,9},{5,13},{9,17},{1... | collective-permute-start | bytes 2359304 | tf_op jit(solution)/shard_map/ppermute | solution.py:358
  (71 other events, 1739.9 us)

commit v2 on v1

--- a/solution.py
+++ b/solution.py
@@ -196,19 +196,35 @@
     )(base, *parts)
 
 
-def expert_kernel(peers, parts, capacity, pad, *refs):
-    line, refs = refs[:parts], refs[parts:]
-    others = [refs[j * parts : (j + 1) * parts] for j in range(peers)]
-    refs = refs[peers * parts :]
-    rank, share, gate, up, down, own = refs[:6]
-    backs = [refs[6 + j * parts : 6 + (j + 1) * parts] for j in range(peers)]
-    packed, made, pick, mixing, shift = refs[6 + peers * parts :]
+def expert_kernel(peers, shape, capacity, pad, *refs):
+    slots = len(shape)
+    lines, others = [], []
+    for parts in shape:
+        lines.append(refs[:parts])
+        refs = refs[parts:]
+    for parts in shape:
+        others.append([refs[j * parts : (j + 1) * parts] for j in range(peers)])
+        refs = refs[peers * parts :]
+    ranks, shares, refs = refs[:slots], refs[slots : 2 * slots], refs[2 * slots :]
+    gate, up, down = refs[:3]
+    owns, refs = refs[3 : 3 + slots], refs[3 + slots :]
+    backs = []
+    for parts in shape:
+        backs.append([refs[j * parts : (j + 1) * parts] for j in range(peers)])
+        refs = refs[peers * parts :]
+    packed, made, pick, mixing, shift = refs
     expert = pl.program_id(0)
     count = pl.num_programs(0)
-    experts = rank.shape[0]
-    rows, span = line[0].shape
-    other_rows = others[0][0].shape[0]
+    experts = ranks[0].shape[0]
+    rows = lines[0][0].shape[0]
+    other_rows = others[0][0][0].shape[0]
     step = 1024
+    group = (1 + peers) * pad
+    filled, width = packed.shape[1:]
+    wide = gate.shape[2]
+
+    def columns(n, skip=0):
+        return pl.ds(pl.multiple_of(skip + n * step, step), step)
 
     @pl.when(expert == 0)
     def _():
@@ -218,48 +234,63 @@
         col = lax.broadcasted_iota(jnp.int32, (pad, other_rows), 1)
         for e in range(experts):
             here = slice(e * pad, (e + 1) * pad)
-            hit = rank[e : e + 1, :] == seat
-            pick[here, :] = hit.astype(f32).astype(bf16)
-            mixing[here, :] = jnp.where(hit, share[e : e + 1, :], 0.0).astype(bf16)
+            for k in range(slots):
+                hit = ranks[k][e : e + 1, :] == seat
+                pick[k, here, :] = hit.astype(f32).astype(bf16)
+                mixing[k, here, :] = jnp.where(hit, shares[k][e : e + 1, :], 0.0).astype(bf16)
             shift[here, :] = (
                 ((col == e * capacity + row) & (row < capacity)).astype(f32).astype(bf16)
             )
-        for h in range(parts):
-
-            def gather(n, carry):
-                at = pl.ds(pl.multiple_of(n * step, step), step)
-                to = pl.ds(pl.multiple_of(h * span + n * step, step), step)
-                for i in range(1 + peers):
-                    source, chooser = (line, pick) if i == 0 else (others[i - 1], shift)
-                    moved = jnp.dot(
-                        chooser[...], source[h][:, at], preferred_element_type=f32
-                    ).astype(bf16)
-                    for e in range(experts):
-                        packed[e, i * pad : (i + 1) * pad, to] = moved[e * pad : (e + 1) * pad]
-                return carry
-
-            lax.fori_loop(0, span // step, gather, 0)
-
-    width = packed.shape[2]
-    wide = gate.shape[2]
-    filled = packed.shape[1]
+        for k, parts in enumerate(shape):
+            span = width // parts
+            for h in range(parts):
+
+                def gather(n, carry):
+                    for i in range(1 + peers):
+                        source = lines[k] if i == 0 else others[k][i - 1]
+                        chooser = pick[k] if i == 0 else shift[...]
+                        moved = jnp.dot(
+                            chooser, source[h][:, columns(n)], preferred_element_type=f32
+                        ).astype(bf16)
+                        at = k * group + i * pad
+                        for e in range(experts):
+                            packed[e, at : at + pad, columns(n, h * span)] = moved[
+                                e * pad : (e + 1) * pad
+                            ]
+                    return carry
+
+                lax.fori_loop(0, span // step, gather, 0)
+
+    even = wide // 256 * 256
+    shared_tile = wide - even == 128 and even > 0
 
     def project(n, carry):
-        at = pl.ds(pl.multiple_of(n * step, step), step)
+        at = columns(n)
         tokens = packed[expert, :, at]
-        return (
-            carry[0] + jnp.dot(tokens, gate[0, at, :], preferred_element_type=f32),
-            carry[1] + jnp.dot(tokens, up[0, at, :], preferred_element_type=f32),
+        if shared_tile:
+            mixed = jnp.concatenate([gate[0, at, even:], up[0, at, :128]], axis=1)
+            blocks = (gate[0, at, :even], mixed, up[0, at, 128:])
+        else:
+            blocks = (gate[0, at, :], up[0, at, :])
+        return tuple(
+            c + jnp.dot(tokens, w, preferred_element_type=f32) for c, w in zip(carry, blocks)
         )
 
-    zero = jnp.zeros((filled, wide), f32)
-    gated, lifted = lax.fori_loop(0, width // step, project, (zero, zero))
+    spans = (even, 256, even) if shared_tile else (wide, wide)
+    sums = lax.fori_loop(
+        0, width // step, project, tuple(jnp.zeros((filled, n), f32) for n in spans)
+    )
+    if shared_tile:
+        gated = jnp.concatenate([sums[0], sums[1][:, :128]], axis=1)
+        lifted = jnp.concatenate([sums[1][:, 128:], sums[2]], axis=1)
+    else:
+        gated, lifted = sums
     hidden = (gated * (1.0 / (1.0 + jnp.exp(-gated))) * lifted).astype(bf16)
 
     def lower(n, carry):
-        at = pl.ds(pl.multiple_of(n * step, step), step)
+        at = columns(n)
         result = jnp.dot(hidden, down[0, :, at], preferred_element_type=f32).astype(bf16)
-        for i in range(1 + peers):
+        for i in range(slots * (1 + peers)):
             made[i, pl.ds(pl.multiple_of(expert * pad, pad), pad), at] = result[
                 i * pad : (i + 1) * pad
             ]
@@ -270,52 +301,60 @@
     @pl.when(expert == count - 1)
     def _():
         rows_in = (((0,), (0,)), ((), ()))
-        for h in range(parts):
-
-            def spread(n, carry):
-                at = pl.ds(pl.multiple_of(n * step, step), step)
-                come = pl.ds(pl.multiple_of(h * span + n * step, step), step)
-                own[:, come] = lax.dot_general(
-                    mixing[...], made[0, :, come], rows_in, preferred_element_type=f32
-                )
-                for j in range(peers):
-                    backs[j][h][:, at] = lax.dot_general(
-                        shift[...], made[1 + j, :, come], rows_in, preferred_element_type=f32
-                    ).astype(bf16)
-                return carry
-
-            lax.fori_loop(0, span // step, spread, 0)
-
-
-def run_experts(line, others, rank, share, gate, up, down, capacity):
-    peers = len(others)
-    parts = len(line)
+        for k, parts in enumerate(shape):
+            span = width // parts
+            for h in range(parts):
+
+                def spread(n, carry):
+                    come = columns(n, h * span)
+                    at = k * (1 + peers)
+                    owns[k][:, come] = lax.dot_general(
+                        mixing[k], made[at, :, come], rows_in, preferred_element_type=f32
+                    )
+                    for j in range(peers):
+                        backs[k][j][h][:, columns(n)] = lax.dot_general(
+                            shift[...],
+                            made[at + 1 + j, :, come],
+                            rows_in,
+                            preferred_element_type=f32,
+                        ).astype(bf16)
+                    return carry
+
+                lax.fori_loop(0, span // step, spread, 0)
+
+
+def run_experts(lines, others, ranks, shares, gate, up, down, capacity):
+    slots = len(lines)
+    peers = len(others[0])
+    shape = tuple(len(line) for line in lines)
     experts, width, hidden = gate.shape
     pad = -(-capacity // 16) * 16
-    rows = line[0].shape[0]
+    rows = lines[0][0].shape[0]
     vm = pl.BlockSpec(memory_space=pltpu.VMEM)
-    flat = [h for group in others for h in group]
+    flat_lines = [h for line in lines for h in line]
+    flat = [h for slot in others for pair in slot for h in pair]
 
     def per_expert(a):
         return pl.BlockSpec((1,) + a.shape[1:], lambda e: (e, 0, 0))
 
-    back_shape = jax.ShapeDtypeStruct(flat[0].shape, bf16)
-    filled = (1 + peers) * pad
+    filled = slots * (1 + peers) * pad
     outs = pl.pallas_call(
-        functools.partial(expert_kernel, peers, parts, capacity, pad),
+        functools.partial(expert_kernel, peers, shape, capacity, pad),
         grid=(experts,),
-        out_shape=[jax.ShapeDtypeStruct((rows, width), f32)] + [back_shape] * len(flat),
-        in_specs=[vm] * (parts + len(flat) + 2) + [per_expert(a) for a in (gate, up, down)],
-        out_specs=[vm] * (1 + len(flat)),
+        out_shape=[jax.ShapeDtypeStruct((rows, width), f32)] * slots
+        + [jax.ShapeDtypeStruct(a.shape, bf16) for a in flat],
+        in_specs=[vm] * (len(flat_lines) + len(flat) + 2 * slots)
+        + [per_expert(a) for a in (gate, up, down)],
+        out_specs=[vm] * (slots + len(flat)),
         scratch_shapes=[
             pltpu.VMEM((experts, filled, width), bf16),
-            pltpu.VMEM((1 + peers, experts * pad, width), bf16),
-            pltpu.VMEM((experts * pad, rows), bf16),
-            pltpu.VMEM((experts * pad, rows), bf16),
+            pltpu.VMEM((slots * (1 + peers), experts * pad, width), bf16),
+            pltpu.VMEM((slots, experts * pad, rows), bf16),
+            pltpu.VMEM((slots, experts * pad, rows), bf16),
             pltpu.VMEM((experts * pad, flat[0].shape[0]), bf16),
         ],
         compiler_params=pltpu.CompilerParams(
-            vmem_limit_bytes=48 * 2**20, dimension_semantics=("arbitrary",)
+            vmem_limit_bytes=56 * 2**20, dimension_semantics=("arbitrary",)
         ),
         cost_estimate=pl.CostEstimate(
             flops=6 * experts * filled * width * hidden,
@@ -323,8 +362,13 @@
             transcendentals=experts * filled * hidden,
         ),
         name="experts",
-    )(*line, *flat, rank, share, gate, up, down)
-    return outs[0], [outs[1 + j * parts : 1 + (j + 1) * parts] for j in range(peers)]
+    )(*flat_lines, *flat, *ranks, *shares, gate, up, down)
+    owns, outs = list(outs[:slots]), outs[slots:]
+    backs = []
+    for parts in shape:
+        backs.append([outs[j * parts : (j + 1) * parts] for j in range(peers)])
+        outs = outs[peers * parts :]
+    return owns, backs
 
 
 def shards(
@@ -502,20 +546,20 @@
         [list(pair) for pair in zip(exchange(3, far[0]), exchange(3, far[1]))],
     ]
     owns, backs = [], []
-    for k in slots:
-        own_table = group_of(k, 0)
-        own, back = run_experts(
-            lines[k],
-            arrived[k],
-            own_table[0],
-            own_table[1],
+    for batch in ((0, 1), (2, 3)):
+        own_tables = [group_of(k, 0) for k in batch]
+        got_own, got_back = run_experts(
+            [lines[k] for k in batch],
+            [arrived[k] for k in batch],
+            [t[0] for t in own_tables],
+            [t[1] for t in own_tables],
             expert_gate,
             expert_up,
             expert_down,
             capacity,
         )
-        owns.append(own)
-        backs.append(back)
+        owns += got_own
+        backs += got_back
 
     def partial_sum(k):
         halves = []

time: 457 us -> 438 us (0.958)
  Pallas kernels: 123 us -> 99.1 us
  starting transfers between devices: 102 us -> 108 us
  other arithmetic: 19.2 us -> 14.4 us
    pallas_call x4 -> x2, Pallas kernels: 85.6 us -> 61.6 us  [run_experts(): pl.pallas_call(functools.partial(expert_kernel, peers, shape, capacity, p...]
    ppermute x27, starting transfers between devices: 79.5 us -> 85.7 us  [along_outer(): return lax.ppermute(x, 'sp', pairs)]
  transfers between devices with their start and end apart: 49 -> 49, of which waited for: 13 -> 16; matrix products, arithmetic and copies ran while one was open for 11% -> 10% of each run, Pallas kernels for 26% -> 22%
where the time goes in v2:
time: 438 us; the launch traced here: 437 us
  waiting for transfers between devices  178 us (41%)
  starting transfers between devices  108 us (25%)
  Pallas kernels  99.1 us (23%)
  matrix products  18.7 us (4%)
  local copies, waits for them, and re-layouts  16.6 us (4%)
  other arithmetic  14.4 us (3%)
    ppermute x27, starting transfers between devices, along_outer(): return lax.ppermute(x, 'sp', pairs)  85.7 us
    ppermute x12, waiting for transfers between devices, along_inner(): return lax.ppermute(x, 'sp', pairs)  74.8 us
    ppermute x27, waiting for transfers between devices, along_outer(): return lax.ppermute(x, 'sp', pairs)  67 us
    pallas_call x2, Pallas kernels, run_experts(): pl.pallas_call(functools.partial(expert_kernel, peers, shape, capacity, p...  61.6 us
    ppermute x8, waiting for transfers between devices, along_tp(): return lax.ppermute(x, 'tp', [(i, i ^ bits) for i in range(n_tp)])  36.6 us
    pallas_call x3, Pallas kernels, out_norm(): pl.pallas_call(functools.partial(out_norm_kernel, blocks, keep, [len(g) f...  23.5 us
    ppermute x12, starting transfers between devices, along_inner(): return lax.ppermute(x, 'sp', pairs)  13.9 us
    pallas_call x8, Pallas kernels, combine(): pl.pallas_call(functools.partial(combine_kernel, count), grid=(2,), out_s...  10.3 us
  transfers between devices with their start and end apart: 49, of which 16 were waited for; matrix products, arithmetic and copies ran while one was open for 10% of the time, Pallas kernels for 22%

profile of v2, /device:TPU:0, one launch (start us, length us, event | category | flops | bytes accessed | tf_op | source)
XLA Modules:
  0.0 436.9 jit_solution(17933664938178026544)
XLA Ops:
  0.0 6.4 %collective-permute-start.18 = (bf16[192,4096]{1,0:T(8,128)(2,1)}, bf16[192,4096]{1,0:T(8,128)(2,1)}, u32[]{:S(2)}, u32[]{:S(2)}) collective-permute-start(bf16[192,4096]{1,0:T(8,128)(2,1)} %refs_2_.1), channel_id=1, source_target_pairs={{0,8},{4,12},{8,16},{12,20},{16,24},{20,28},{1,9},{5,13},{9,17},{1... | collective-permute-start | bytes 4718600 | tf_op jit(solution)/shard_map/ppermute | solution.py:402
  8.4 3.4 collective-permute-start
  23.4 3.2 collective-permute-done.4
  26.5 25.5 %collective-permute-start.29 = (f32[2,8,192]{2,1,0:T(8,128)S(1)}, f32[2,8,192]{2,1,0:T(8,128)S(1)}, u32[]{:S(2)}, u32[]{:S(2)}) collective-permute-start(f32[2,8,192]{2,1,0:T(8,128)S(1)} %get-tuple-element.57), channel_id=1, source_target_pairs={{0,16},{4,20},{8,24},{12,28},{16,0},{20,4},{24,8},{28,12},{1,17},{... | collective-permute-start | bytes 36872 | tf_op jit(solution)/shard_map/ppermute | solution.py:402
  52.1 3.2 collective-permute-start.14
  57.4 5.3 %collective-permute-start.13 = (bf16[192,1024]{1,0:T(8,128)(2,1)S(1)}, bf16[192,1024]{1,0:T(8,128)(2,1)}, u32[]{:S(2)}, u32[]{:S(2)}) collective-permute-start(bf16[192,1024]{1,0:T(8,128)(2,1)S(1)} %pad_maximum_fusion.refs_0_), channel_id=1, source_target_pairs={{0,8},{4,12},{8,16},{12,20},{16,24},{20,28},{1,9},{5,13},{9,17},{1... | collective-permute-start | bytes 1179656 | tf_op jit(solution)/shard_map/ppermute | solution.py:402
  63.0 5.3 %collective-permute-done.12 = bf16[192,1024]{1,0:T(8,128)(2,1)} collective-permute-done((bf16[192,1024]{1,0:T(8,128)(2,1)S(1)}, bf16[192,1024]{1,0:T(8,128)(2,1)}, u32[]{:S(2)}, u32[]{:S(2)}) %collective-permute-start.12) | collective-permute-done | bytes 393248 | tf_op jit(solution)/shard_map/ppermute | solution.py:402
  74.7 5.6 %collective-permute-done.22 = bf16[192,1024]{1,0:T(8,128)(2,1)} collective-permute-done((bf16[192,1024]{1,0:T(8,128)(2,1)}, bf16[192,1024]{1,0:T(8,128)(2,1)}, u32[]{:S(2)}, u32[]{:S(2)}) %collective-permute-start.22) | collective-permute-done | bytes 393248 | tf_op jit(solution)/shard_map/ppermute | solution.py:402
  84.4 13.2 %collective-permute-done.9.refs_8_.refs_10_.refs_6_ = bf16[256,2048]{1,0:T(8,128)(2,1)} collective-permute-done((bf16[256,2048]{1,0:T(8,128)(2,1)}, bf16[256,2048]{1,0:T(8,128)(2,1)}, u32[]{:S(2)}, u32[]{:S(2)}) %collective-permute-start.9) | collective-permute-done | bytes 1048608 | tf_op jit(solution)/shard_map/ppermute | solution.py:413
  97.6 20.3 %collective-permute-done.8.refs_7_.refs_9_.refs_5_ = bf16[256,2048]{1,0:T(8,128)(2,1)} collective-permute-done((bf16[256,2048]{1,0:T(8,128)(2,1)}, bf16[256,2048]{1,0:T(8,128)(2,1)}, u32[]{:S(2)}, u32[]{:S(2)}) %collective-permute-start.8) | collective-permute-done | bytes 1048608 | tf_op jit(solution)/shard_map/ppermute | solution.py:413
  125.5 31.8 %collective-permute-done.24 = bf16[192,4096]{1,0:T(8,128)(2,1)S(1)} collective-permute-done((bf16[192,4096]{1,0:T(8,128)(2,1)}, bf16[192,4096]{1,0:T(8,128)(2,1)S(1)}, u32[]{:S(2)}, u32[]{:S(2)}) %collective-permute-start.24) | collective-permute-done | bytes 1572896 | tf_op jit(solution)/shard_map/ppermute | solution.py:402
  160.1 5.1 %out_norm.5.refs_0_ = bf16[192,4096]{1,0:T(8,128)(2,1)S(1)} custom-call(bf16[192,1024]{1,0:T(8,128)(2,1)S(1)} %add.322.refs_0_, bf16[192,4096]{1,0:T(8,128)(2,1)S(1)} %add.323.refs_1_, f32[1,4096]{1,0:T(1,128)S(1)} %bitcast.86, bf16[256,4096]{1,0:T(8,128)(2,1)S(1)} %copy-done.2, bf16[256,4096]{1,0:T(8,128)(2,1)S(1)} %collective-permute-done.7.refs_6_.refs_8_.refs_4_, ...), custom_call_target="tpu_custom_call" | custom-call | flops 1610612736 | bytes 3145728 | tf_op jit(solution)/shard_map/out_norm/pallas_call | solution.py:125
  167.6 24.1 %collective-permute-done.16.refs_2_ = bf16[144,1024]{1,0:T(8,128)(2,1)S(1)} collective-permute-done((bf16[144,1024]{1,0:T(8,128)(2,1)S(1)}, bf16[144,1024]{1,0:T(8,128)(2,1)S(1)}, u32[]{:S(2)}, u32[]{:S(2)}) %collective-permute-start.16) | collective-permute-done | bytes 294944 | tf_op jit(solution)/shard_map/ppermute | solution.py:410
  194.0 10.5 %out_norm.4 = (bf16[192,4096]{1,0:T(8,128)(2,1)S(1)}, bf16[192,4096]{1,0:T(8,128)(2,1)S(1)}, bf16[144,4096]{1,0:T(8,128)(2,1)S(1)}) custom-call(bf16[192,1024]{1,0:T(8,128)(2,1)S(1)} %get-tuple-element.50.refs_0_, bf16[192,1024]{1,0:T(8,128)(2,1)S(1)} %get-tuple-element.49.refs_1_, bf16[144,1024]{1,0:T(8,128)(2,1)S(1)} %collective-permute-done.16.refs_2_, ...), custom_call_target="tpu_custom_call" | custom-call | flops 4429185024 | bytes 8650752 | tf_op jit(solution)/shard_map/out_norm/pallas_call | solution.py:125
  208.8 16.1 %collective-permute-done.28 = bf16[192,2048]{1,0:T(8,128)(2,1)S(1)} collective-permute-done((bf16[192,2048]{1,0:T(8,128)(2,1)S(1)}, bf16[192,2048]{1,0:T(8,128)(2,1)S(1)}, u32[]{:S(2)}, u32[]{:S(2)}) %collective-permute-start.28) | collective-permute-done | bytes 786464 | tf_op jit(solution)/shard_map/ppermute | solution.py:402
  230.0 6.3 %collective-permute-done.30.refs_3_ = bf16[144,4096]{1,0:T(8,128)(2,1)} collective-permute-done((bf16[144,4096]{1,0:T(8,128)(2,1)S(1)}, bf16[144,4096]{1,0:T(8,128)(2,1)}, u32[]{:S(2)}, u32[]{:S(2)}) %collective-permute-start.30) | collective-permute-done | bytes 1179680 | tf_op jit(solution)/shard_map/ppermute | solution.py:410
  236.3 12.5 %collective-permute-done.31.refs_4_ = bf16[144,2048]{1,0:T(8,128)(2,1)S(1)} collective-permute-done((bf16[144,2048]{1,0:T(8,128)(2,1)S(1)}, bf16[144,2048]{1,0:T(8,128)(2,1)S(1)}, u32[]{:S(2)}, u32[]{:S(2)}) %collective-permute-start.31) | collective-permute-done | bytes 589856 | tf_op jit(solution)/shard_map/ppermute | solution.py:410
  248.8 10.7 %collective-permute-done.32.refs_5_ = bf16[144,2048]{1,0:T(8,128)(2,1)S(1)} collective-permute-done((bf16[144,2048]{1,0:T(8,128)(2,1)S(1)}, bf16[144,2048]{1,0:T(8,128)(2,1)S(1)}, u32[]{:S(2)}, u32[]{:S(2)}) %collective-permute-start.32) | collective-permute-done | bytes 589856 | tf_op jit(solution)/shard_map/ppermute | solution.py:410
  260.4 30.7 %experts.3 = (f32[192,4096]{1,0:T(8,128)}, f32[192,4096]{1,0:T(8,128)}, bf16[144,4096]{1,0:T(8,128)(2,1)}, bf16[144,2048]{1,0:T(8,128)(2,1)}, bf16[144,2048]{1,0:T(8,128)(2,1)}) custom-call(bf16[192,4096]{1,0:T(8,128)(2,1)} %copy-done.1, bf16[192,2048]{1,0:T(8,128)(2,1)} %copy-done.26, bf16[192,2048]{1,0:T(8,128)(2,1)} %copy-done.27, ...), custom_call_target="tpu_custom_call" | custom-call | flops 7247757312 | bytes 37748736 | tf_op jit(solution)/shard_map/experts/pallas_call | solution.py:341
  298.3 9.2 %collective-permute-done.33.refs_1_ = bf16[144,2048]{1,0:T(8,128)(2,1)S(1)} collective-permute-done((bf16[144,2048]{1,0:T(8,128)(2,1)}, bf16[144,2048]{1,0:T(8,128)(2,1)S(1)}, u32[]{:S(2)}, u32[]{:S(2)}) %collective-permute-start.33) | collective-permute-done | bytes 589856 | tf_op jit(solution)/shard_map/ppermute | solution.py:410
  313.9 5.2 %collective-permute-start.36 = (bf16[192,2048]{1,0:T(8,128)(2,1)S(1)}, bf16[192,2048]{1,0:T(8,128)(2,1)}, u32[]{:S(2)}, u32[]{:S(2)}) collective-permute-start(bf16[192,2048]{1,0:T(8,128)(2,1)S(1)} %combine.10), channel_id=1, source_target_pairs={{0,8},{4,12},{1,9},{5,13},{2,10},{6,14},{3,11},{7,15}} | collective-permute-start | bytes 2359304 | tf_op jit(solution)/shard_map/ppermute | solution.py:402
  319.2 7.9 %out_norm.3 = (bf16[192,4096]{1,0:T(8,128)(2,1)S(1)}, bf16[144,4096]{1,0:T(8,128)(2,1)S(1)}, bf16[192,4096]{1,0:T(8,128)(2,1)S(1)}) custom-call(bf16[192,1024]{1,0:T(8,128)(2,1)S(1)} %copy-done.19, bf16[144,1024]{1,0:T(8,128)(2,1)S(1)} %collective-permute-done.5.refs_1_, bf16[192,4096]{1,0:T(8,128)(2,1)S(1)} %copy-done.12, ...), custom_call_target="tpu_custom_call" | custom-call | flops 2818572288 | bytes 5505024 | tf_op jit(solution)/shard_map/out_norm/pallas_call | solution.py:125
  330.2 4.0 collective-permute-start.41
  334.2 30.9 %experts.2 = (f32[192,4096]{1,0:T(8,128)}, f32[192,4096]{1,0:T(8,128)}, bf16[144,4096]{1,0:T(8,128)(2,1)}, bf16[144,4096]{1,0:T(8,128)(2,1)}) custom-call(bf16[192,4096]{1,0:T(8,128)(2,1)} %copy-done.3, bf16[192,4096]{1,0:T(8,128)(2,1)} %copy-done.17, bf16[144,4096]{1,0:T(8,128)(2,1)} %copy-done.22, bf16[144,4096]{1,0:T(8,128)(2,1)} %copy-done.21, ...), custom_call_target="tpu_custom_call" | custom-call | flops 7247757312 | bytes 37748736 | tf_op jit(solution)/shard_map/experts/pallas_call | solution.py:341
  375.9 5.1 %collective-permute-start.43 = (bf16[192,2048]{1,0:T(8,128)(2,1)S(1)}, bf16[192,2048]{1,0:T(8,128)(2,1)S(1)}, u32[]{:S(2)}, u32[]{:S(2)}) collective-permute-start(bf16[192,2048]{1,0:T(8,128)(2,1)S(1)} %add_add_fusion), channel_id=1, source_target_pairs={{0,8},{4,12},{8,16},{12,20},{1,9},{5,13},{9,17},{13,21},{2,10},{6,... | collective-permute-start | bytes 2359304 | tf_op jit(solution)/shard_map/ppermute | solution.py:402
  381.2 10.0 %collective-permute-done.34.refs_1_ = bf16[144,4096]{1,0:T(8,128)(2,1)S(1)} collective-permute-done((bf16[144,4096]{1,0:T(8,128)(2,1)}, bf16[144,4096]{1,0:T(8,128)(2,1)S(1)}, u32[]{:S(2)}, u32[]{:S(2)}) %collective-permute-start.34) | collective-permute-done | bytes 1179680 | tf_op jit(solution)/shard_map/ppermute | solution.py:410
  397.1 5.7 %collective-permute-start.39 = (bf16[192,2048]{1,0:T(8,128)(2,1)}, bf16[192,2048]{1,0:T(8,128)(2,1)}, u32[]{:S(2)}, u32[]{:S(2)}) collective-permute-start(bf16[192,2048]{1,0:T(8,128)(2,1)} %get-tuple-element.46), channel_id=1, source_target_pairs={{0,8},{4,12},{8,16},{12,20},{16,24},{20,28},{1,9},{5,13},{9,17},{1... | collective-permute-start | bytes 2359304 | tf_op jit(solution)/shard_map/ppermute | solution.py:402
  402.8 3.7 collective-permute-done.43
  409.1 5.9 %collective-permute-start.44 = (bf16[192,2048]{1,0:T(8,128)(2,1)}, bf16[192,2048]{1,0:T(8,128)(2,1)}, u32[]{:S(2)}, u32[]{:S(2)}) collective-permute-start(bf16[192,2048]{1,0:T(8,128)(2,1)} %get-tuple-element.44), channel_id=1, source_target_pairs={{0,8},{4,12},{8,16},{12,20},{16,24},{20,28},{1,9},{5,13},{9,17},{1... | collective-permute-start | bytes 2359304 | tf_op jit(solution)/shard_map/ppermute | solution.py:402
  416.8 6.5 %convert_add_fusion.base = f32[192,4096]{1,0:T(8,128)} fusion(bf16[192,4096]{1,0:T(8,128)(2,1)} %copy-done.20, bf16[384,4096]{1,0:T(8,128)(2,1)S(1)} %copy-done, f32[192,384]{1,0:T(8,128)} %fusion.53, bf16[192,4096]{1,0:T(8,128)(2,1)} %copy-done.3, bf16[4096,384]{1,0:T(8,128)(2,1)} %param.26), kind=kOutput, calls=%fused_computation.3 | convolution fusion | flops 1209974784 | bytes 12877824 | tf_op jit(solution)/shard_map/dot_general | solution.py:585
  428.8 4.5 %collective-permute-done.44.up_b = bf16[192,2048]{1,0:T(8,128)(2,1)} collective-permute-done((bf16[192,2048]{1,0:T(8,128)(2,1)}, bf16[192,2048]{1,0:T(8,128)(2,1)}, u32[]{:S(2)}, u32[]{:S(2)}) %collective-permute-start.44) | collective-permute-done | bytes 786464 | tf_op jit(solution)/shard_map/ppermute | solution.py:402
  433.2 3.7 finish.1
  (249 shorter events, 94.1 us)
Async XLA Ops:
  0.0 82.7 %collective-permute-start.18 = (bf16[192,4096]{1,0:T(8,128)(2,1)}, bf16[192,4096]{1,0:T(8,128)(2,1)}, u32[]{:S(2)}, u32[]{:S(2)}) collective-permute-start(bf16[192,4096]{1,0:T(8,128)(2,1)} %refs_2_.1), channel_id=1, source_target_pairs={{0,8},{4,12},{8,16},{12,20},{16,24},{20,28},{1,9},{5,13},{9,17},{1... | collective-permute-start | bytes 4718600 | tf_op jit(solution)/shard_map/ppermute | solution.py:402
  6.4 111.5 %collective-permute-start.17 = (bf16[192,4096]{1,0:T(8,128)(2,1)}, bf16[192,4096]{1,0:T(8,128)(2,1)}, u32[]{:S(2)}, u32[]{:S(2)}) collective-permute-start(bf16[192,4096]{1,0:T(8,128)(2,1)} %refs_2_.1), channel_id=1, source_target_pairs={{24,16},{28,20},{16,8},{20,12},{8,0},{12,4},{25,17},{29,21},{17,9}... | collective-permute-start | bytes 4718600 | tf_op jit(solution)/shard_map/ppermute | solution.py:402
  21.8 30.2 %collective-permute-start.3 = (bf16[192,256]{1,0:T(8,128)(2,1)S(1)}, bf16[192,256]{1,0:T(8,128)(2,1)S(1)}, u32[]{:S(2)}, u32[]{:S(2)}) collective-permute-start(bf16[192,256]{1,0:T(8,128)(2,1)S(1)} %get-tuple-element.53), channel_id=1, source_target_pairs={{0,2},{1,3},{2,0},{3,1},{4,6},{5,7},{6,4},{7,5},{8,10},{9,11},{10,... | collective-permute-start | bytes 294920 | tf_op jit(solution)/shard_map/ppermute | solution.py:413
  23.0 32.2 %collective-permute-start.2 = (bf16[192,256]{1,0:T(8,128)(2,1)S(1)}, bf16[192,256]{1,0:T(8,128)(2,1)S(1)}, u32[]{:S(2)}, u32[]{:S(2)}) collective-permute-start(bf16[192,256]{1,0:T(8,128)(2,1)S(1)} %get-tuple-element.54), channel_id=1, source_target_pairs={{0,1},{1,0},{2,3},{3,2},{4,5},{5,4},{6,7},{7,6},{8,9},{9,8},{10,11... | collective-permute-start | bytes 294920 | tf_op jit(solution)/shard_map/ppermute | solution.py:413
  26.5 30.8 %collective-permute-start.29 = (f32[2,8,192]{2,1,0:T(8,128)S(1)}, f32[2,8,192]{2,1,0:T(8,128)S(1)}, u32[]{:S(2)}, u32[]{:S(2)}) collective-permute-start(f32[2,8,192]{2,1,0:T(8,128)S(1)} %get-tuple-element.57), channel_id=1, source_target_pairs={{0,16},{4,20},{8,24},{12,28},{16,0},{20,4},{24,8},{28,12},{1,17},{... | collective-permute-start | bytes 36872 | tf_op jit(solution)/shard_map/ppermute | solution.py:402
  71.2 26.3 %collective-permute-start.9 = (bf16[256,2048]{1,0:T(8,128)(2,1)}, bf16[256,2048]{1,0:T(8,128)(2,1)}, u32[]{:S(2)}, u32[]{:S(2)}) collective-permute-start(bf16[256,2048]{1,0:T(8,128)(2,1)} %get-tuple-element.41), channel_id=1, source_target_pairs={{0,2},{1,3},{2,0},{3,1},{4,6},{5,7},{6,4},{7,5},{8,10},{9,11},{10,... | collective-permute-start | bytes 3145736 | tf_op jit(solution)/shard_map/ppermute | solution.py:413
  71.6 46.3 %collective-permute-start.8 = (bf16[256,2048]{1,0:T(8,128)(2,1)}, bf16[256,2048]{1,0:T(8,128)(2,1)}, u32[]{:S(2)}, u32[]{:S(2)}) collective-permute-start(bf16[256,2048]{1,0:T(8,128)(2,1)} %get-tuple-element.42), channel_id=1, source_target_pairs={{0,2},{1,3},{2,0},{3,1},{4,6},{5,7},{6,4},{7,5},{8,10},{9,11},{10,... | collective-permute-start | bytes 3145736 | tf_op jit(solution)/shard_map/ppermute | solution.py:413
  81.9 78.1 %collective-permute-start.7 = (bf16[256,4096]{1,0:T(8,128)(2,1)}, bf16[256,4096]{1,0:T(8,128)(2,1)S(1)}, u32[]{:S(2)}, u32[]{:S(2)}) collective-permute-start(bf16[256,4096]{1,0:T(8,128)(2,1)} %refs_3_.1), channel_id=1, source_target_pairs={{0,1},{1,0},{2,3},{3,2},{4,5},{5,4},{6,7},{7,6},{8,9},{9,8},{10,11... | collective-permute-start | bytes 6291464 | tf_op jit(solution)/shard_map/ppermute | solution.py:413
  82.8 39.0 %collective-permute-start.23 = (bf16[192,4096]{1,0:T(8,128)(2,1)}, bf16[192,4096]{1,0:T(8,128)(2,1)S(1)}, u32[]{:S(2)}, u32[]{:S(2)}) collective-permute-start(bf16[192,4096]{1,0:T(8,128)(2,1)} %collective-permute-done.18), channel_id=1, source_target_pairs={{8,16},{12,20},{16,24},{20,28},{9,17},{13,21},{17,25},{21,29},{10,... | collective-permute-start | bytes 4718600 | tf_op jit(solution)/shard_map/ppermute | solution.py:402
  97.6 61.7 %collective-permute-start.11 = (bf16[256,2048]{1,0:T(8,128)(2,1)}, bf16[256,2048]{1,0:T(8,128)(2,1)S(1)}, u32[]{:S(2)}, u32[]{:S(2)}) collective-permute-start(bf16[256,2048]{1,0:T(8,128)(2,1)} %collective-permute-done.9.refs_8_.refs_10_.refs_6_), channel_id=1, source_target_pairs={{0,1},{1,0},{2,3},{3,2},{4,5},{5,4},{6,7},{7,6},{8,9},{9,8},{10,11... | collective-permute-start | bytes 3145736 | tf_op jit(solution)/shard_map/ppermute | solution.py:413
  117.8 42.2 %collective-permute-start.10 = (bf16[256,2048]{1,0:T(8,128)(2,1)}, bf16[256,2048]{1,0:T(8,128)(2,1)S(1)}, u32[]{:S(2)}, u32[]{:S(2)}) collective-permute-start(bf16[256,2048]{1,0:T(8,128)(2,1)} %collective-permute-done.8.refs_7_.refs_9_.refs_5_), channel_id=1, source_target_pairs={{0,1},{1,0},{2,3},{3,2},{4,5},{5,4},{6,7},{7,6},{8,9},{9,8},{10,11... | collective-permute-start | bytes 3145736 | tf_op jit(solution)/shard_map/ppermute | solution.py:413
  117.8 39.5 %collective-permute-start.24 = (bf16[192,4096]{1,0:T(8,128)(2,1)}, bf16[192,4096]{1,0:T(8,128)(2,1)S(1)}, u32[]{:S(2)}, u32[]{:S(2)}) collective-permute-start(bf16[192,4096]{1,0:T(8,128)(2,1)} %collective-permute-done.17), channel_id=1, source_target_pairs={{16,8},{20,12},{8,0},{12,4},{17,9},{21,13},{9,1},{13,5},{18,10},{2... | collective-permute-start | bytes 4718600 | tf_op jit(solution)/shard_map/ppermute | solution.py:402
  121.7 70.0 %collective-permute-start.19 = (bf16[144,4096]{1,0:T(8,128)(2,1)S(1)}, bf16[144,4096]{1,0:T(8,128)(2,1)S(1)}, u32[]{:S(2)}, u32[]{:S(2)}) collective-permute-start(bf16[144,4096]{1,0:T(8,128)(2,1)S(1)} %convolution_convert_fusion.1), channel_id=1, source_target_pairs={{0,4},{4,0},{8,12},{12,8},{16,20},{20,16},{24,28},{28,24},{1,5},{5... | collective-permute-start | bytes 3538952 | tf_op jit(solution)/shard_map/ppermute | solution.py:410
  157.4 161.8 %collective-permute-start.6 = (bf16[144,4096]{1,0:T(8,128)(2,1)}, bf16[144,4096]{1,0:T(8,128)(2,1)}, u32[]{:S(2)}, u32[]{:S(2)}) collective-permute-start(bf16[144,4096]{1,0:T(8,128)(2,1)} %convolution_convert_fusion.2), channel_id=1, source_target_pairs={{0,4},{4,0},{8,12},{12,8},{16,20},{20,16},{24,28},{28,24},{1,5},{5... | collective-permute-start | bytes 3538952 | tf_op jit(solution)/shard_map/ppermute | solution.py:410
  159.3 32.4 %collective-permute-start.16 = (bf16[144,1024]{1,0:T(8,128)(2,1)S(1)}, bf16[144,1024]{1,0:T(8,128)(2,1)S(1)}, u32[]{:S(2)}, u32[]{:S(2)}) collective-permute-start(bf16[144,1024]{1,0:T(8,128)(2,1)S(1)} %convolution_convert_fusion.5), channel_id=1, source_target_pairs={{0,4},{4,0},{8,12},{12,8},{16,20},{20,16},{24,28},{28,24},{1,5},{5... | collective-permute-start | bytes 884744 | tf_op jit(solution)/shard_map/ppermute | solution.py:410
  165.3 41.9 %collective-permute-start.26 = (bf16[192,2048]{1,0:T(8,128)(2,1)S(1)}, bf16[192,2048]{1,0:T(8,128)(2,1)S(1)}, u32[]{:S(2)}, u32[]{:S(2)}) collective-permute-start(bf16[192,2048]{1,0:T(8,128)(2,1)S(1)} %get-tuple-element.48), channel_id=1, source_target_pairs={{8,0},{12,4},{9,1},{13,5},{10,2},{14,6},{11,3},{15,7}} | collective-permute-start | bytes 2359304 | tf_op jit(solution)/shard_map/ppermute | solution.py:402
  166.6 42.1 %collective-permute-start.25 = (bf16[192,2048]{1,0:T(8,128)(2,1)S(1)}, bf16[192,2048]{1,0:T(8,128)(2,1)S(1)}, u32[]{:S(2)}, u32[]{:S(2)}) collective-permute-start(bf16[192,2048]{1,0:T(8,128)(2,1)S(1)} %get-tuple-element.48), channel_id=1, source_target_pairs={{16,24},{20,28},{17,25},{21,29},{18,26},{22,30},{19,27},{23,31}} | collective-permute-start | bytes 2359304 | tf_op jit(solution)/shard_map/ppermute | solution.py:402
  207.3 29.0 %collective-permute-start.30 = (bf16[144,4096]{1,0:T(8,128)(2,1)S(1)}, bf16[144,4096]{1,0:T(8,128)(2,1)}, u32[]{:S(2)}, u32[]{:S(2)}) collective-permute-start(bf16[144,4096]{1,0:T(8,128)(2,1)S(1)} %convolution_convert_fusion), channel_id=1, source_target_pairs={{0,4},{4,0},{8,12},{12,8},{16,20},{20,16},{24,28},{28,24},{1,5},{5... | collective-permute-start | bytes 3538952 | tf_op jit(solution)/shard_map/ppermute | solution.py:410
  227.2 32.3 %collective-permute-start.32 = (bf16[144,2048]{1,0:T(8,128)(2,1)S(1)}, bf16[144,2048]{1,0:T(8,128)(2,1)S(1)}, u32[]{:S(2)}, u32[]{:S(2)}) collective-permute-start(bf16[144,2048]{1,0:T(8,128)(2,1)S(1)} %convolution_convert_fusion.3), channel_id=1, source_target_pairs={{0,4},{4,0},{8,12},{12,8},{16,20},{20,16},{24,28},{28,24},{1,5},{5... | collective-permute-start | bytes 1769480 | tf_op jit(solution)/shard_map/ppermute | solution.py:410
  295.5 31.6 %collective-permute-start.40 = (bf16[144,2048]{1,0:T(8,128)(2,1)S(1)}, bf16[144,2048]{1,0:T(8,128)(2,1)S(1)}, u32[]{:S(2)}, u32[]{:S(2)}) collective-permute-start(bf16[144,2048]{1,0:T(8,128)(2,1)S(1)} %copy-done.55), channel_id=1, source_target_pairs={{0,4},{4,0},{8,12},{12,8},{16,20},{20,16},{24,28},{28,24},{1,5},{5... | collective-permute-start | bytes 1769480 | tf_op jit(solution)/shard_map/ppermute | solution.py:410
  297.5 67.6 %collective-permute-start.35 = (bf16[144,4096]{1,0:T(8,128)(2,1)}, bf16[144,4096]{1,0:T(8,128)(2,1)}, u32[]{:S(2)}, u32[]{:S(2)}) collective-permute-start(bf16[144,4096]{1,0:T(8,128)(2,1)} %get-tuple-element.37), channel_id=1, source_target_pairs={{0,4},{4,0},{8,12},{12,8},{16,20},{20,16},{24,28},{28,24},{1,5},{5... | collective-permute-start | bytes 3538952 | tf_op jit(solution)/shard_map/ppermute | solution.py:410
  310.3 57.9 %collective-permute-start.37 = (bf16[192,2048]{1,0:T(8,128)(2,1)S(1)}, bf16[192,2048]{1,0:T(8,128)(2,1)}, u32[]{:S(2)}, u32[]{:S(2)}) collective-permute-start(bf16[192,2048]{1,0:T(8,128)(2,1)S(1)} %combine.10), channel_id=1, source_target_pairs={{24,16},{28,20},{25,17},{29,21},{26,18},{30,22},{27,19},{31,23}} | collective-permute-start | bytes 2359304 | tf_op jit(solution)/shard_map/ppermute | solution.py:402
  313.9 54.3 %collective-permute-start.36 = (bf16[192,2048]{1,0:T(8,128)(2,1)S(1)}, bf16[192,2048]{1,0:T(8,128)(2,1)}, u32[]{:S(2)}, u32[]{:S(2)}) collective-permute-start(bf16[192,2048]{1,0:T(8,128)(2,1)S(1)} %combine.10), channel_id=1, source_target_pairs={{0,8},{4,12},{1,9},{5,13},{2,10},{6,14},{3,11},{7,15}} | collective-permute-start | bytes 2359304 | tf_op jit(solution)/shard_map/ppermute | solution.py:402
  328.6 44.9 %collective-permute-start.42 = (bf16[192,2048]{1,0:T(8,128)(2,1)S(1)}, bf16[192,2048]{1,0:T(8,128)(2,1)}, u32[]{:S(2)}, u32[]{:S(2)}) collective-permute-start(bf16[192,2048]{1,0:T(8,128)(2,1)S(1)} %combine.13), channel_id=1, source_target_pairs={{24,16},{28,20},{25,17},{29,21},{26,18},{30,22},{27,19},{31,23}} | collective-permute-start | bytes 2359304 | tf_op jit(solution)/shard_map/ppermute | solution.py:402
  330.2 43.4 %collective-permute-start.41 = (bf16[192,2048]{1,0:T(8,128)(2,1)S(1)}, bf16[192,2048]{1,0:T(8,128)(2,1)}, u32[]{:S(2)}, u32[]{:S(2)}) collective-permute-start(bf16[192,2048]{1,0:T(8,128)(2,1)S(1)} %combine.13), channel_id=1, source_target_pairs={{0,8},{4,12},{1,9},{5,13},{2,10},{6,14},{3,11},{7,15}} | collective-permute-start | bytes 2359304 | tf_op jit(solution)/shard_map/ppermute | solution.py:402
  365.1 26.2 %collective-permute-start.34 = (bf16[144,4096]{1,0:T(8,128)(2,1)}, bf16[144,4096]{1,0:T(8,128)(2,1)S(1)}, u32[]{:S(2)}, u32[]{:S(2)}) collective-permute-start(bf16[144,4096]{1,0:T(8,128)(2,1)} %get-tuple-element.35), channel_id=1, source_target_pairs={{0,4},{4,0},{8,12},{12,8},{16,20},{20,16},{24,28},{28,24},{1,5},{5... | collective-permute-start | bytes 3538952 | tf_op jit(solution)/shard_map/ppermute | solution.py:410
  369.7 24.6 %collective-permute-start.45 = (bf16[192,2048]{1,0:T(8,128)(2,1)S(1)}, bf16[192,2048]{1,0:T(8,128)(2,1)S(1)}, u32[]{:S(2)}, u32[]{:S(2)}) collective-permute-start(bf16[192,2048]{1,0:T(8,128)(2,1)S(1)} %add_add_fusion.1), channel_id=1, source_target_pairs={{24,16},{28,20},{16,8},{20,12},{25,17},{29,21},{17,9},{21,13},{26,... | collective-permute-start | bytes 2359304 | tf_op jit(solution)/shard_map/ppermute | solution.py:402
  375.2 27.6 %collective-permute-start.47 = (bf16[192,2048]{1,0:T(8,128)(2,1)S(1)}, bf16[192,2048]{1,0:T(8,128)(2,1)S(1)}, u32[]{:S(2)}, u32[]{:S(2)}) collective-permute-start(bf16[192,2048]{1,0:T(8,128)(2,1)S(1)} %add_add_fusion), channel_id=1, source_target_pairs={{24,16},{28,20},{16,8},{20,12},{25,17},{29,21},{17,9},{21,13},{26,... | collective-permute-start | bytes 2359304 | tf_op jit(solution)/shard_map/ppermute | solution.py:402
  375.9 30.6 %collective-permute-start.43 = (bf16[192,2048]{1,0:T(8,128)(2,1)S(1)}, bf16[192,2048]{1,0:T(8,128)(2,1)S(1)}, u32[]{:S(2)}, u32[]{:S(2)}) collective-permute-start(bf16[192,2048]{1,0:T(8,128)(2,1)S(1)} %add_add_fusion), channel_id=1, source_target_pairs={{0,8},{4,12},{8,16},{12,20},{1,9},{5,13},{9,17},{13,21},{2,10},{6,... | collective-permute-start | bytes 2359304 | tf_op jit(solution)/shard_map/ppermute | solution.py:402
  391.3 32.0 %collective-permute-start.20 = (bf16[144,4096]{1,0:T(8,128)(2,1)}, bf16[144,4096]{1,0:T(8,128)(2,1)}, u32[]{:S(2)}, u32[]{:S(2)}) collective-permute-start(bf16[144,4096]{1,0:T(8,128)(2,1)} %get-tuple-element.28), channel_id=1, source_target_pairs={{0,4},{4,0},{8,12},{12,8},{16,20},{20,16},{24,28},{28,24},{1,5},{5... | collective-permute-start | bytes 3538952 | tf_op jit(solution)/shard_map/ppermute | solution.py:410
  395.8 33.0 %collective-permute-start.46 = (bf16[192,2048]{1,0:T(8,128)(2,1)}, bf16[192,2048]{1,0:T(8,128)(2,1)}, u32[]{:S(2)}, u32[]{:S(2)}) collective-permute-start(bf16[192,2048]{1,0:T(8,128)(2,1)} %get-tuple-element.45), channel_id=1, source_target_pairs={{24,16},{28,20},{16,8},{20,12},{8,0},{12,4},{25,17},{29,21},{17,9}... | collective-permute-start | bytes 2359304 | tf_op jit(solution)/shard_map/ppermute | solution.py:402
  397.1 31.7 %collective-permute-start.39 = (bf16[192,2048]{1,0:T(8,128)(2,1)}, bf16[192,2048]{1,0:T(8,128)(2,1)}, u32[]{:S(2)}, u32[]{:S(2)}) collective-permute-start(bf16[192,2048]{1,0:T(8,128)(2,1)} %get-tuple-element.46), channel_id=1, source_target_pairs={{0,8},{4,12},{8,16},{12,20},{16,24},{20,28},{1,9},{5,13},{9,17},{1... | collective-permute-start | bytes 2359304 | tf_op jit(solution)/shard_map/ppermute | solution.py:402
  (75 other events, 1613.7 us)
